TPU v7x, 32 devices: a whole 2x2x4 slice. The times are simulated.
32 devices in a mesh: grp: 2 (over y), ep: 8 (over z, core), tp: 2 (over x).
Axes of the slice: x: 2, y: 2, z: 4, core: 2. Of those that a mesh axis runs over, the one named last changes fastest.
Arguments:
- recurrence_query_input: bfloat16 [2048, 2048], P(('grp', 'ep'), 'tp'), parts along dimension 0, may hold values from -6 to 6
- forget_gate_input: bfloat16 [2048, 2048], P(('grp', 'ep'), 'tp'), parts along dimension 0, may hold values from -6.5 to 6.5
- recurrence_value_input: bfloat16 [2048, 2048], P(('grp', 'ep'), 'tp'), parts along dimension 0, may hold values from -6 to 6
- output_gate_input: bfloat16 [2048, 2048], P(('grp', 'ep'), 'tp'), parts along dimension 0, may hold values from -6 to 6
- forget_lower_margin: float32 [2048], P('tp'), may hold values from 0 to 0.1
- position_decay_extra: float32 [2048, 16], P(('grp', 'ep'), 'tp'), parts along dimension 0, may hold values from -2.1 to 0
- head_norm_gain: float32 [2048], P('tp'), may hold values from 0.1 to 1.9
- recurrence_out_weight: bfloat16 [2048, 2048], P('tp'), may hold values from -0.125 to 0.125
- expert_hidden_state: bfloat16 [2048, 2048], P(('grp', 'ep')), parts along dimension 0, may hold values from -6 to 6
- chosen_expert_index: int32 [2048, 4], P(('grp', 'ep')), parts along dimension 0, may hold values from 0 to 7, all different within a row; in each aligned block of 128 rows (0 to 127, 128 to 255, ...) at most 128 rows name the same one
- chosen_expert_score: float32 [2048, 4], P(('grp', 'ep')), parts along dimension 0, may hold values from 0.02 to 1
- expert_norm_gain: float32 [2048], replicated, may hold values from 0.1 to 1.9
- routed_gate_weight: bfloat16 [8, 2048, 1024], P('ep', None, 'tp'), may hold values from -0.125 to 0.125
- routed_up_weight: bfloat16 [8, 2048, 1024], P('ep', None, 'tp'), may hold values from -0.125 to 0.125
- routed_down_weight: bfloat16 [8, 1024, 2048], P('ep', None, 'tp'), may hold values from -0.1875 to 0.1875
- shared_gate_weight: bfloat16 [2048, 1024], P(None, 'tp'), may hold values from -0.125 to 0.125
- shared_up_weight: bfloat16 [2048, 1024], P(None, 'tp'), may hold values from -0.125 to 0.125
- shared_down_weight: bfloat16 [1024, 2048], P(None, 'tp'), may hold values from -0.1875 to 0.1875
Outputs:
- recurrence_output: bfloat16 [2048, 2048], P(('grp', 'ep', 'tp')), parts along dimension 0
- expert_out: bfloat16 [2048, 2048], P(('grp', 'ep'), 'tp'), parts along dimension 0
There are 2 independent parts, one for each index of `grp`. A program takes and returns all parts, laid end to end along the dimension named above; an argument that names none is the same for every part. Nothing has to cross between parts.
Inputs may be any that keep to these rules, and one draw needn't show every extreme that they name: `chosen_expert_index`: each row names 4 different experts. In each aligned block of 128 rows (the rows of one index of ep) no expert is named by more than 128 rows, and in every draw some block names some expert exactly 128 times.
All inputs are finite; a program needn't handle non-finite values.
Results may differ from a plain program's by a relative error of at most 0.015.
Values may be sent and summed in bfloat16 or wider, within the bound.
A program may use at most 64 MiB of HBM per device.

v0:
```python
import jax
import jax.numpy as jnp
from jax import lax
from jax.sharding import PartitionSpec as P

HEAD_CHANNELS = 128
BLK = 64


EPSILON = 1e-06
ROUTED_SCALE = 2.5
HIGHEST_PRECISION = lax.Precision.HIGHEST


def carried_in(array, axis, combine, identity):
    count, index = (lax.axis_size(axis), lax.axis_index(axis))
    everything = jax.tree.map(
        lambda part, kind: lax.all_gather(part.astype(kind), axis),
        array,
        (jnp.bfloat16, jnp.bfloat16),
    )
    start = jax.tree.map(
        lambda part, zero: jnp.broadcast_to(jnp.asarray(zero, part.dtype), part.shape),
        array,
        identity,
    )

    def turn(k, before):
        reached = k < index
        new = combine(
            before, jax.tree.map(lambda part, own: part[k].astype(own.dtype), everything, array)
        )
        return jax.tree.map(lambda a, b: jnp.where(reached, a, b), new, before)

    return lax.fori_loop(0, count, turn, start)


def chain_states(earlier, later):
    return (earlier[0] * later[0], later[0][..., None] * earlier[1] + later[1])


def mixer_half(
    recurrence_query_input,
    forget_gate_input,
    recurrence_value_input,
    output_gate_input,
    forget_lower_margin,
    position_decay_extra,
    head_norm_gain,
    recurrence_out_weight,
):
    length = recurrence_query_input.shape[0]
    head_tensor = position_decay_extra.shape[1]
    blocks = length // BLK
    queries = jax.nn.silu(recurrence_query_input.astype(jnp.float32))
    key_gate_value = forget_lower_margin[None, :] * jax.nn.sigmoid(
        -forget_gate_input.astype(jnp.float32)
    )
    decay_logarithm = jnp.log1p(-key_gate_value) + jnp.repeat(
        position_decay_extra, HEAD_CHANNELS, axis=1
    )
    value_rows = recurrence_value_input.astype(jnp.float32)

    def split_heads(tensor):
        return tensor.reshape(blocks, BLK, head_tensor, HEAD_CHANNELS).transpose(2, 0, 1, 3)

    query_heads = split_heads(queries)
    key_heads = split_heads(key_gate_value)
    value_heads = split_heads(value_rows)
    cum_decay = jnp.cumsum(split_heads(decay_logarithm), axis=2)
    middle = cum_decay[:, :, BLK // 2 - 1 : BLK // 2]
    block_end = cum_decay[:, :, BLK - 1 : BLK]
    scores = jnp.einsum(
        "hncd,hnsd->hncs",
        query_heads * jnp.exp(cum_decay - middle),
        key_heads * jnp.exp(middle - cum_decay),
        precision=HIGHEST_PRECISION,
    )
    causal = jnp.tril(jnp.ones((BLK, BLK), dtype=bool))
    scores = jnp.where(causal, scores, 0.0)
    within = jnp.einsum("hncs,hnse->hnce", scores, value_heads, precision=HIGHEST_PRECISION)
    updates = jnp.einsum(
        "hncd,hnce->nhde",
        key_heads * jnp.exp(block_end - cum_decay),
        value_heads,
        precision=HIGHEST_PRECISION,
    )
    block_log = block_end[:, :, 0, :]
    block_decay = jnp.exp(block_log).transpose(1, 0, 2)

    def advance(carry_state, inputs):
        factor, update = inputs
        return (factor[..., None] * carry_state + update, carry_state)

    initial = jnp.zeros((head_tensor, HEAD_CHANNELS, HEAD_CHANNELS), jnp.float32)
    local_final, local_starts = lax.scan(advance, initial, (block_decay, updates))
    device_decay = jnp.exp(jnp.sum(block_log, axis=1))
    identity = (jnp.ones_like(device_decay), jnp.zeros_like(local_final))
    _, incoming = carried_in((device_decay, local_final), "ep", chain_states, identity)
    before = jnp.exp(jnp.cumsum(block_log, axis=1) - block_log).transpose(1, 0, 2)
    starts = local_starts + before[..., None] * incoming[None]
    carried = jnp.einsum(
        "hncd,nhde->hnce", query_heads * jnp.exp(cum_decay), starts, precision=HIGHEST_PRECISION
    )
    outputs = (within + carried).transpose(1, 2, 0, 3).reshape(length, head_tensor, HEAD_CHANNELS)
    factor = lax.rsqrt(jnp.mean(outputs * outputs, axis=2, keepdims=True) + EPSILON)
    normed = (outputs * factor).reshape(length, head_tensor * HEAD_CHANNELS) * head_norm_gain[
        None, :
    ]
    gated_rows = (normed * jax.nn.silu(output_gate_input.astype(jnp.float32))).astype(jnp.bfloat16)
    return lax.psum_scatter(
        jnp.dot(gated_rows, recurrence_out_weight, preferred_element_type=jnp.float32).astype(
            jnp.bfloat16
        ),
        "tp",
        scatter_dimension=0,
        tiled=True,
    )


def expert_half(
    expert_hidden_state,
    chosen_expert_index,
    chosen_expert_score,
    expert_norm_gain,
    routed_gate_weight,
    routed_up_weight,
    routed_down_weight,
    shared_gate_weight,
    shared_up_weight,
    shared_down_weight,
):
    tokens, top = chosen_expert_index.shape
    local_experts = routed_gate_weight.shape[0]
    devices = lax.axis_size("ep")
    experts = local_experts * devices
    capacity = min(tokens, 2 * tokens * top // experts)
    width_out = routed_down_weight.shape[2]
    features = expert_hidden_state.astype(jnp.float32)
    normed = (
        features
        * lax.rsqrt(jnp.mean(features * features, axis=1, keepdims=True) + EPSILON)
        * expert_norm_gain[None, :]
    ).astype(jnp.bfloat16)
    gates = ROUTED_SCALE * chosen_expert_score / jnp.sum(chosen_expert_score, axis=1, keepdims=True)
    flat_ids = chosen_expert_index.reshape(-1)
    onehot = (flat_ids[:, None] == jnp.arange(experts, dtype=jnp.int32)[None, :]).astype(jnp.int32)
    places = jnp.sum(onehot * (jnp.cumsum(onehot, axis=0) - 1), axis=1)
    slots = flat_ids * capacity + places
    owners = (
        jnp.full((experts * capacity,), tokens, jnp.int32)
        .at[slots]
        .set(jnp.arange(tokens * top, dtype=jnp.int32) // top)
    )
    padded = jnp.concatenate([normed, jnp.zeros((1, normed.shape[1]), jnp.bfloat16)], axis=0)
    outgoing = padded[owners].reshape(experts, capacity, normed.shape[1])
    piece = lax.all_to_all(outgoing, "ep", split_axis=0, concat_axis=0, tiled=True)
    grouped = piece.reshape(devices, local_experts, piece.shape[1], piece.shape[2])
    gate_part = jnp.einsum(
        "secd,edh->sech", grouped, routed_gate_weight, preferred_element_type=jnp.float32
    )
    up_part = jnp.einsum(
        "secd,edh->sech", grouped, routed_up_weight, preferred_element_type=jnp.float32
    )
    hidden = (jax.nn.silu(gate_part) * up_part).astype(jnp.bfloat16)
    hidden_rows = hidden.reshape(devices * local_experts, piece.shape[1], hidden.shape[3])
    flat_hidden = hidden_rows.reshape(experts * capacity, hidden_rows.shape[2])
    shared_hidden = (
        jax.nn.silu(jnp.dot(normed, shared_gate_weight, preferred_element_type=jnp.float32))
        * jnp.dot(normed, shared_up_weight, preferred_element_type=jnp.float32)
    ).astype(jnp.bfloat16)
    start_values = (
        jnp.zeros((experts * capacity, width_out), jnp.float32),
        jnp.zeros((tokens, width_out), jnp.float32),
    )
    routed_piece = lax.all_gather(flat_hidden, "tp", axis=1, tiled=True)
    shared_piece = lax.all_gather(shared_hidden, "tp", axis=1, tiled=True)
    count = routed_piece.shape[1]
    grouped = routed_piece.reshape(devices, local_experts, capacity, count)
    routed = jnp.einsum(
        "secn,enk->seck", grouped, routed_down_weight, preferred_element_type=jnp.float32
    )
    shared = jnp.dot(shared_piece, shared_down_weight, preferred_element_type=jnp.float32)
    routed_sum = routed.reshape(start_values[0].shape)
    answers = routed_sum.astype(jnp.bfloat16).reshape(experts, capacity, width_out)
    returned = lax.all_to_all(answers, "ep", split_axis=0, concat_axis=0, tiled=True)
    picked_rows = returned.reshape(experts * capacity, width_out)[slots].reshape(
        tokens, top, width_out
    )
    combined = shared + jnp.sum(gates[:, :, None] * picked_rows.astype(jnp.float32), axis=1)
    return combined.astype(jnp.bfloat16)


def per_device(
    recurrence_query_input,
    forget_gate_input,
    recurrence_value_input,
    output_gate_input,
    forget_lower_margin,
    position_decay_extra,
    head_norm_gain,
    recurrence_out_weight,
    expert_hidden_state,
    chosen_expert_index,
    chosen_expert_score,
    expert_norm_gain,
    routed_gate_weight,
    routed_up_weight,
    routed_down_weight,
    shared_gate_weight,
    shared_up_weight,
    shared_down_weight,
):
    recurrence_output = mixer_half(
        recurrence_query_input,
        forget_gate_input,
        recurrence_value_input,
        output_gate_input,
        forget_lower_margin,
        position_decay_extra,
        head_norm_gain,
        recurrence_out_weight,
    )
    expert_out = expert_half(
        expert_hidden_state,
        chosen_expert_index,
        chosen_expert_score,
        expert_norm_gain,
        routed_gate_weight,
        routed_up_weight,
        routed_down_weight,
        shared_gate_weight,
        shared_up_weight,
        shared_down_weight,
    )
    return (recurrence_output, expert_out)


def solution(mesh):
    in_specs = (
        P(("grp", "ep"), "tp"),
        P(("grp", "ep"), "tp"),
        P(("grp", "ep"), "tp"),
        P(("grp", "ep"), "tp"),
        P("tp"),
        P(("grp", "ep"), "tp"),
        P("tp"),
        P("tp", None),
        P(("grp", "ep"), None),
        P(("grp", "ep"), None),
        P(("grp", "ep"), None),
        P(),
        P("ep", None, "tp"),
        P("ep", None, "tp"),
        P("ep", None, "tp"),
        P(None, "tp"),
        P(None, "tp"),
        P(None, "tp"),
    )
    out_specs = (P(("grp", "ep", "tp"), None), P(("grp", "ep"), "tp"))
    return jax.shard_map(
        per_device, mesh=mesh, in_specs=in_specs, out_specs=out_specs, check_vma=False
    )
```

profile of v0, /device:TPU:0, one launch (start us, length us, event | category | flops | bytes accessed | tf_op | source)
XLA Modules:
  0.0 260.2 jit_solution(11099438260719906569)
XLA Ops:
  12.0 2.4 scatter_custom_fusion
  15.8 6.0 %gather_fusion = bf16[1024,2048]{1,0:T(8,128)(2,1)} fusion(bf16[129,2048]{1,0:T(8,128)(2,1)S(1)} %concatenate.3, s32[1024]{0:T(1024)S(1)} %fusion.54), kind=kCustom, calls=%fused_computation | custom fusion | bytes 8392704 | tf_op jit(solution)/shard_map/gather | solution.py:156
  21.8 6.5 %all-to-all-start = ((bf16[8,128,2048]{2,1,0:T(8,128)(2,1)}), bf16[8,128,2048]{2,1,0:T(8,128)(2,1)}, u32[]{:S(2)}, u32[]{:S(2)}) async-start(bf16[8,128,2048]{2,1,0:T(8,128)(2,1)} %bitcast.170), calls=%async_computation.1 | async-start | bytes 8388608 | tf_op jit(solution)/shard_map/all_to_all | solution.py:157
  31.1 91.3 %all-to-all-done = bf16[8,128,2048]{2,1,0:T(8,128)(2,1)} async-done(((bf16[8,128,2048]{2,1,0:T(8,128)(2,1)}), bf16[8,128,2048]{2,1,0:T(8,128)(2,1)}, u32[]{:S(2)}, u32[]{:S(2)}) %all-to-all-start) | async-done | bytes 4194336 | tf_op jit(solution)/shard_map/all_to_all | solution.py:157
  122.4 5.3 %fusion.4 = f32[8,128,512]{2,1,0:T(8,128)S(1)} fusion(bf16[8,128,2048]{2,1,0:T(8,128)(2,1)} %all-to-all-done, bf16[1,2048,512]{2,1,0:T(8,128)(2,1)} %param.35), kind=kOutput, calls=%fused_computation.14 | convolution fusion | flops 2147483648 | bytes 8388608 | tf_op jit(solution)/shard_map/secd,edh->sech/dot_general | solution.py:162
  127.7 5.9 %fusion.1 = bf16[8,1,128,512]{3,2,0,1:T(8,128)(2,1)} fusion(f32[8,128,512]{2,1,0:T(8,128)S(1)} %fusion.4, bf16[8,128,2048]{2,1,0:T(8,128)(2,1)} %all-to-all-done, bf16[1,2048,512]{2,1,0:T(8,128)(2,1)S(1)} %copy-done.11), kind=kOutput, calls=%fused_computation.11 | convolution fusion | flops 2150629376 | bytes 9437184 | tf_op jit(solution)/shard_map/secd,edh->sech/dot_general | solution.py:159
  137.1 1.3 bitcast_multiply_fusion.3
  138.4 2.0 fusion.38
  140.4 4.4 %while.27 = (s32[]{:T(128)}, f32[8,128,128]{2,1,0:T(8,128)S(1)}, f32[2,8,128,128]{3,2,1,0:T(8,128)}, f32[2,8,128]{2,1,0:T(8,128)S(1)}, f32[2,8,128,128]{3,2,1,0:T(8,128)}, /*index=5*/s32[]{:T(128)}, s32[]{:T(128)}) while((s32[]{:T(128)}, f32[8,128,128]{2,1,0:T(8,128)S(1)}, f32[2,8,128,128]{3,2,1,0:T(8,128)}, ...), condition=%wide.region_2.3_spmd.clone, body=%wide.region_1.2_spmd.clone.sunk | while | flops 524291 | bytes 2633836 | solution.py:96
  141.2 1.4 bitcast_add_fusion.3
  143.5 1.3 bitcast_add_fusion.3
  145.6 13.1 %all-gather = bf16[64,128]{1,0:T(8,128)(2,1)S(1)} all-gather(bf16[8,128]{1,0:T(8,128)(2,1)S(1)} %exponential_convert_fusion), channel_id=2, replica_groups=mesh['grp'=2,'ep'=8,'tp'=2] {'ep'}, dimensions={0}, use_global_device_ids=true | all-gather | bytes 18432 | tf_op jit(solution)/shard_map/all_gather | solution.py:18
  159.6 2.4 convolution_select_fusion
  164.4 1.3 all-gather.5.cloned.1.call-done
  165.8 5.2 %fusion.11 = bf16[8,128,1024]{2,1,0:T(8,128)(2,1)} fusion(bf16[8,128,1024]{2,1,0:T(8,128)(2,1)} %bitcast.187, bf16[1,1024,1024]{2,1,0:T(8,128)(2,1)S(1)} %copy-done), kind=kOutput, calls=%fused_computation.24 | convolution fusion | flops 2148532224 | bytes 6291456 | tf_op jit(solution)/shard_map/secn,enk->seck/dot_general | solution.py:180
  171.0 4.6 %all-to-all-start.1 = ((bf16[8,128,1024]{2,1,0:T(8,128)(2,1)}), bf16[8,128,1024]{2,1,0:T(8,128)(2,1)}, u32[]{:S(2)}, u32[]{:S(2)}) async-start(bf16[8,128,1024]{2,1,0:T(8,128)(2,1)} %fusion.11), calls=%async_computation.2 | async-start | bytes 4194304 | tf_op jit(solution)/shard_map/all_to_all | solution.py:186
  175.6 38.3 %all-gather.7.cloned.1.call-done = bf16[64,128,128]{2,1,0:T(8,128)(2,1)} async-done(((bf16[8,128,128]{2,1,0:T(8,128)(2,1)}), bf16[64,128,128]{2,1,0:T(8,128)(2,1)}) %all-gather.7.cloned.1.call-update) | async-done | bytes 2097168 | tf_op jit(solution)/shard_map/all_gather | solution.py:18
  214.0 10.7 %while.28 = (s32[]{:T(128)}, f32[8,128,128]{2,1,0:T(8,128)S(1)}, s32[]{:T(128)}, bf16[8,8,128]{2,1,0:T(8,128)(2,1)S(1)}, bf16[8,8,128,128]{3,2,1,0:T(8,128)(2,1)}, /*index=5*/s32[]{:T(128)}, s32[]{:T(128)}) while((s32[]{:T(128)}, f32[8,128,128]{2,1,0:T(8,128)S(1)}, s32[]{:T(128)}, bf16[8,8,128]{2,1,0:T(8,128)(2,1)S(1)}, ...), condition=%wide.region_6.7_spmd.clone, body=%wide.region_5.6_spmd.clone.sunk | while | flops 656388 | bytes 1321073 | solution.py:35
  215.3 1.3 fusion.77
  216.7 1.3 fusion.77
  218.0 1.3 fusion.77
  219.3 1.3 fusion.77
  220.7 1.3 fusion.77
  222.0 1.3 fusion.77
  224.7 3.6 %multiply_reduce_fusion.1 = (f32[2,64,8]{1,0,2:T(2,128)S(1)}, f32[2,64,8,128]{3,1,0,2:T(8,128)}) fusion(f32[8,2,64,128]{3,2,1,0:T(8,128)} %fusion.45, f32[8,2,64,128]{3,0,1,2:T(8,128)} %get-tuple-element.188, f32[2,8,128,128]{3,2,1,0:T(8,128)} %get-tuple-element.124, f32[8,128,128]{2,1,0:T(8,128)S(1)} %get-tuple-element.126, f32[2,8,128]{2,1,0:T(8,128)S(1)} %fusion.20), kind=kOutput, calls=%fused_computation.70 | convolution fusion | flops 202243072 | bytes 3158016 | tf_op jit(solution)/shard_map/hncd,nhde->hnce/dot_general | solution.py:102
  228.4 1.4 copy.53
  230.0 4.0 %convolution_convert_fusion = bf16[128,2048]{1,0:T(8,128)(2,1)} fusion(bf16[1024,2048]{1,0:T(8,128)(2,1)} %param.29, bf16[128,1024]{1,0:T(8,128)(2,1)} %param.25, f32[16,8,8,128]{3,2,1,0:T(8,128)S(1)} %bitcast.179, f32[16,8,8,128]{3,2,1,0:T(8,128)S(1)} %bitcast.180, f32[1024]{0:T(1024)S(1)} %copy-done.12), kind=kOutput, calls=%fused_computation.9 | convolution fusion | flops 538312704 | bytes 6033408 | tf_op jit(solution)/shard_map/dot_general | solution.py:112
  234.1 2.0 fusion.18
  236.2 6.6 %all_gather.19 = bf16[128,1024]{1,0:T(8,128)(2,1)S(1)} all-gather(bf16[128,512]{1,0:T(8,128)(2,1)S(1)} %fusion.18), channel_id=1, replica_groups=mesh['grp'=2,'ep'=8,'tp'=2] {'tp'}, dimensions={1}, use_global_device_ids=true | all-gather | bytes 393216 | tf_op jit(solution)/shard_map/all_gather | solution.py:177
  242.8 4.6 %gather_fusion.1 = bf16[512,1024]{1,0:T(8,128)(2,1)S(1)} fusion(bf16[1024,1024]{1,0:T(8,128)(2,1)} %bitcast.34, s32[1024]{0:T(1024)S(1)} %pad_clamp_fusion), kind=kCustom, calls=%fused_computation.1 | custom fusion | bytes 2099200 | tf_op jit(solution)/shard_map/gather | solution.py:187
  247.4 1.7 reshape.179
  249.1 3.1 %multiply_reduce_fusion = f32[128,1024]{1,0:T(8,128)S(1)} fusion(f32[128,4,1024]{2,1,0:T(4,128)} %reshape.179, f32[128,4]{1,0:T(8,128)S(1)} %copy.55), kind=kLoop, calls=%fused_computation.23 | loop fusion | flops 917504 | bytes 2623488 | tf_op jit(solution)/shard_map/reduce_sum | solution.py:190
  (96 shorter events, 22.5 us)
Async XLA Ops:
  7.2 158.6 %copy-start = (bf16[1,1024,1024]{2,1,0:T(8,128)(2,1)S(1)}, bf16[1,1024,1024]{2,1,0:T(8,128)(2,1)}, u32[]{:S(2)}) copy-start(bf16[1,1024,1024]{2,1,0:T(8,128)(2,1)} %param.36) | copy-start | bytes 6291460
  21.8 6.6 %copy-start.10 = (f32[128,8]{0,1:T(8,128)S(1)}, f32[128,8]{0,1:T(8,128)}, u32[]{:S(2)}) copy-start(f32[128,8]{0,1:T(8,128)} %param.27) | copy-start | bytes 12292
  21.8 6.9 %copy-start.5 = (bf16[128,1024]{1,0:T(8,128)(2,1)S(1)}, bf16[128,1024]{1,0:T(8,128)(2,1)}, u32[]{:S(2)}) copy-start(bf16[128,1024]{1,0:T(8,128)(2,1)} %param.23) | copy-start | bytes 786436
  21.8 6.9 %copy-start.9 = (f32[1024]{0:T(1024)S(1)}, f32[1024]{0:T(1024)}, u32[]{:S(2)}) copy-start(f32[1024]{0:T(1024)} %param.26) | copy-start | bytes 12292
  21.8 100.6 %all-to-all-start = ((bf16[8,128,2048]{2,1,0:T(8,128)(2,1)}), bf16[8,128,2048]{2,1,0:T(8,128)(2,1)}, u32[]{:S(2)}, u32[]{:S(2)}) async-start(bf16[8,128,2048]{2,1,0:T(8,128)(2,1)} %bitcast.170), calls=%async_computation.1 | async-start | bytes 8388608 | tf_op jit(solution)/shard_map/all_to_all | solution.py:157
  28.3 1.6 copy-start.6
  28.3 137.5 %all-gather.5.cloned.1.call-start = ((), (), s32[]{:S(2)}) async-start(), calls=%async_computation.4 | async-start | bytes 3145728 | tf_op jit(solution)/shard_map/all_gather | solution.py:176
  31.0 102.6 %copy-start.1 = (f32[8,2,64,128]{3,0,1,2:T(8,128)}, f32[8,2,64,128]{3,0,1,2:T(8,128)S(1)}, u32[]{:S(2)}) copy-start(f32[8,2,64,128]{3,0,1,2:T(8,128)S(1)} %fusion.35) | copy-start | bytes 1572868
  122.4 5.3 %copy-start.11 = (bf16[1,2048,512]{2,1,0:T(8,128)(2,1)S(1)}, bf16[1,2048,512]{2,1,0:T(8,128)(2,1)}, u32[]{:S(2)}) copy-start(bf16[1,2048,512]{2,1,0:T(8,128)(2,1)} %param.34) | copy-start | bytes 6291460
  133.6 80.4 %all-gather.7.cloned.1.call-start = ((), (), s32[]{:S(2)}) async-start(), calls=%async_computation.5 | async-start | bytes 2359296 | tf_op jit(solution)/shard_map/all_gather | solution.py:18
  133.7 3.4 %copy-start.2 = (f32[8,2,64,128]{3,0,1,2:T(8,128)S(1)}, f32[8,2,64,128]{3,0,1,2:T(8,128)}, u32[]{:S(2)}) copy-start(f32[8,2,64,128]{3,0,1,2:T(8,128)} %copy-done.1) | copy-start | bytes 1572868
  140.4 5.2 %copy-start.8 = (f32[128,4]{0,1:T(4,128)S(1)}, f32[128,4]{0,1:T(4,128)}, u32[]{:S(2)}) copy-start(f32[128,4]{0,1:T(4,128)} %param.32) | copy-start | bytes 6148
  145.6 17.6 %copy-start.4 = (bf16[2048,512]{1,0:T(8,128)(2,1)S(1)}, bf16[2048,512]{1,0:T(8,128)(2,1)}, u32[]{:S(2)}) copy-start(bf16[2048,512]{1,0:T(8,128)(2,1)} %param.37) | copy-start | bytes 6291460
  171.0 71.8 %all-to-all-start.1 = ((bf16[8,128,1024]{2,1,0:T(8,128)(2,1)}), bf16[8,128,1024]{2,1,0:T(8,128)(2,1)}, u32[]{:S(2)}, u32[]{:S(2)}) async-start(bf16[8,128,1024]{2,1,0:T(8,128)(2,1)} %fusion.11), calls=%async_computation.2 | async-start | bytes 4194304 | tf_op jit(solution)/shard_map/all_to_all | solution.py:186
  175.6 78.1 %reduce-scatter.2.cloned.1.call-start = ((), (), s32[]{:S(2)}) async-start(), calls=%async_computation.3 | async-start | bytes 786432 | tf_op jit(solution)/shard_map/reduce_scatter | solution.py:111
  224.7 5.3 %copy-start.12 = (f32[1024]{0:T(1024)S(1)}, f32[1024]{0:T(1024)}, u32[]{:S(2)}) copy-start(f32[1024]{0:T(1024)} %param.28) | copy-start | bytes 12292
  230.0 4.2 %copy-start.7 = (f32[128,512]{1,0:T(8,128)S(1)}, f32[128,512]{1,0:T(8,128)}, u32[]{:S(2)}) copy-start(f32[128,512]{1,0:T(8,128)} %fusion.61) | copy-start | bytes 786436
  249.1 3.1 %copy-start.3 = (bf16[1024,1024]{1,0:T(8,128)(2,1)S(1)}, bf16[1024,1024]{1,0:T(8,128)(2,1)}, u32[]{:S(2)}) copy-start(bf16[1024,1024]{1,0:T(8,128)(2,1)} %param.39) | copy-start | bytes 6291460
Sparse Core Ops, SparseCore 0:
  133.7 32.0 all-gather.4
  167.9 45.9 all-gather.6
  234.1 19.4 reduce-scatter.1
where the time goes:
time: 264 us; the launch traced here: 260 us
  waiting for transfers between devices  131 us (50%)
  matrix products  34 us (13%)
  other arithmetic  27.7 us (10%)
  local copies, waits for them, and re-layouts  21.8 us (8%)
  blocking collectives  19.7 us (7%)
  between operations  14.1 us (5%)
  starting transfers between devices  11.2 us (4%)
    all_to_all x1, waiting for transfers between devices, expert_half(): lax.all_to_all(outgoing, 'ep', split_axis=0, concat_axis=0, tiled=True)  91.3 us
    all_gather x1, waiting for transfers between devices, carried_in(): lax.all_gather(part.astype(kind), axis)  38.3 us
    all_gather x1, blocking collectives, carried_in(): lax.all_gather(part.astype(kind), axis)  13.1 us
    select_n x8, other arithmetic, turn(): return jax.tree.map(lambda a, b: jnp.where(reached, a, b), new, before)  10.4 us
    all_gather x1, blocking collectives, expert_half(): shared_piece = lax.all_gather(shared_hidden, 'tp', axis=1, tiled=True)  6.58 us
    all_to_all x1, starting transfers between devices, expert_half(): lax.all_to_all(outgoing, 'ep', split_axis=0, concat_axis=0, tiled=True)  6.49 us
    gather x1, local copies, waits for them, and re-layouts, expert_half(): outgoing = padded[owners].reshape(experts, capacity, normed.shape[1])  6.03 us
    dot_general x1, matrix products, expert_half(): jnp.einsum('secd,edh->sech', grouped, routed_gate_weight, preferred_eleme...  5.86 us
  transfers between devices with their start and end apart: 5, of which 4 were waited for; matrix products, arithmetic and copies ran while one was open for 22% of the time, Pallas kernels for 0%

commit v1 on v0

--- a/solution.py
+++ b/solution.py
@@ -9,7 +9,7 @@
 
 EPSILON = 1e-06
 ROUTED_SCALE = 2.5
-HIGHEST_PRECISION = lax.Precision.HIGHEST
+PRECISION = lax.Precision.DEFAULT
 
 
 def carried_in(array, axis, combine, identity):
@@ -74,16 +74,16 @@
         "hncd,hnsd->hncs",
         query_heads * jnp.exp(cum_decay - middle),
         key_heads * jnp.exp(middle - cum_decay),
-        precision=HIGHEST_PRECISION,
+        precision=PRECISION,
     )
     causal = jnp.tril(jnp.ones((BLK, BLK), dtype=bool))
     scores = jnp.where(causal, scores, 0.0)
-    within = jnp.einsum("hncs,hnse->hnce", scores, value_heads, precision=HIGHEST_PRECISION)
+    within = jnp.einsum("hncs,hnse->hnce", scores, value_heads, precision=PRECISION)
     updates = jnp.einsum(
         "hncd,hnce->nhde",
         key_heads * jnp.exp(block_end - cum_decay),
         value_heads,
-        precision=HIGHEST_PRECISION,
+        precision=PRECISION,
     )
     block_log = block_end[:, :, 0, :]
     block_decay = jnp.exp(block_log).transpose(1, 0, 2)
@@ -100,7 +100,7 @@
     before = jnp.exp(jnp.cumsum(block_log, axis=1) - block_log).transpose(1, 0, 2)
     starts = local_starts + before[..., None] * incoming[None]
     carried = jnp.einsum(
-        "hncd,nhde->hnce", query_heads * jnp.exp(cum_decay), starts, precision=HIGHEST_PRECISION
+        "hncd,nhde->hnce", query_heads * jnp.exp(cum_decay), starts, precision=PRECISION
     )
     outputs = (within + carried).transpose(1, 2, 0, 3).reshape(length, head_tensor, HEAD_CHANNELS)
     factor = lax.rsqrt(jnp.mean(outputs * outputs, axis=2, keepdims=True) + EPSILON)
@@ -189,6 +189,55 @@
     )
     combined = shared + jnp.sum(gates[:, :, None] * picked_rows.astype(jnp.float32), axis=1)
     return combined.astype(jnp.bfloat16)
+
+
+def dense_expert_half(
+    expert_hidden_state,
+    chosen_expert_index,
+    chosen_expert_score,
+    expert_norm_gain,
+    routed_gate_weight,
+    routed_up_weight,
+    routed_down_weight,
+    shared_gate_weight,
+    shared_up_weight,
+    shared_down_weight,
+):
+    tokens, top = chosen_expert_index.shape
+    experts = lax.axis_size("ep")
+    features = expert_hidden_state.astype(jnp.float32)
+    width = features.shape[1]
+    normed = (
+        features
+        * lax.rsqrt(jnp.mean(features * features, axis=1, keepdims=True) + EPSILON)
+        * expert_norm_gain[None, :]
+    ).astype(jnp.bfloat16)
+    gates = ROUTED_SCALE * chosen_expert_score / jnp.sum(chosen_expert_score, axis=1, keepdims=True)
+    chosen = chosen_expert_index[:, :, None] == jnp.arange(64, dtype=jnp.int32)[None, None, :]
+    gate_table = jnp.sum(jnp.where(chosen, gates[:, :, None], 0.0), axis=1)
+    high = gate_table.astype(jnp.bfloat16)
+    low = (gate_table - high.astype(jnp.float32)).astype(jnp.bfloat16)
+    sent = jnp.concatenate([normed, high, low], axis=1)
+    everything = lax.all_gather(sent, "ep", axis=0, tiled=True)
+    rows = everything[:, :width]
+    mine = jnp.arange(64, dtype=jnp.int32) == lax.axis_index("ep")
+    tail = everything[:, width:].astype(jnp.float32)
+    own_gate = jnp.sum(jnp.where(mine[None, :], tail[:, :64] + tail[:, 64:], 0.0), axis=1)
+    shared_hidden = (
+        jax.nn.silu(jnp.dot(normed, shared_gate_weight, preferred_element_type=jnp.float32))
+        * jnp.dot(normed, shared_up_weight, preferred_element_type=jnp.float32)
+    ).astype(jnp.bfloat16)
+    gate_part = jnp.dot(rows, routed_gate_weight[0], preferred_element_type=jnp.float32)
+    up_part = jnp.dot(rows, routed_up_weight[0], preferred_element_type=jnp.float32)
+    hidden = (jax.nn.silu(gate_part) * up_part * own_gate[:, None]).astype(jnp.bfloat16)
+    shared_full = lax.all_gather(shared_hidden, "tp", axis=1, tiled=True)
+    hidden_full = lax.all_gather(hidden, "tp", axis=1, tiled=True)
+    shared = jnp.dot(shared_full, shared_down_weight, preferred_element_type=jnp.float32)
+    routed = jnp.dot(
+        hidden_full, routed_down_weight[0], preferred_element_type=jnp.float32
+    ).astype(jnp.bfloat16)
+    total = lax.psum_scatter(routed, "ep", scatter_dimension=0, tiled=True)
+    return (shared + total.astype(jnp.float32)).astype(jnp.bfloat16)
 
 
 def per_device(
@@ -221,7 +270,11 @@
         head_norm_gain,
         recurrence_out_weight,
     )
-    expert_out = expert_half(
+    tokens, top = chosen_expert_index.shape
+    experts = routed_gate_weight.shape[0] * lax.axis_size("ep")
+    every_row_fits = 2 * top >= experts and routed_gate_weight.shape[0] == 1 and experts <= 64
+    half = dense_expert_half if every_row_fits else expert_half
+    expert_out = half(
         expert_hidden_state,
         chosen_expert_index,
         chosen_expert_score,

time: 264 us -> 199 us (0.75); the launches traced: 260 us -> 198 us
  waiting for transfers between devices: 131 us -> 98.3 us
  local copies, waits for them, and re-layouts: 21.8 us -> 8.28 us
  starting transfers between devices: 11.2 us -> 0.2 us
  matrix products: 34 us -> 29.8 us
    all_to_all x2 -> x0, waiting for transfers between devices: 91.3 us -> none  [the longest x1 91.3 us: expert_half(): lax.all_to_all(outgoing, 'ep', split_axis=0, concat_axis=0, tiled=True)]
    all_gather x1 -> x2, waiting for transfers between devices: 1.34 us -> 53.4 us  [the longest x1 46.3 us: dense_expert_half(): everything = lax.all_gather(sent, 'ep', axis=0, tiled=True)]
    all_gather x1, waiting for transfers between devices: 38.3 us -> 22.4 us  [carried_in(): lax.all_gather(part.astype(kind), axis)]
    reduce_scatter x1, waiting for transfers between devices: 0.23 us -> 13 us  [mixer_half(): lax.psum_scatter(jnp.dot(gated_rows, recurrence_out_weight, preferred_ele...]
    all_to_all x2 -> x0, starting transfers between devices: 11.1 us -> none  [the longest x1 6.49 us: expert_half(): lax.all_to_all(outgoing, 'ep', split_axis=0, concat_axis=0, tiled=True)]
    gather x2 -> x0, local copies, waits for them, and re-layouts: 10.6 us -> none  [the longest x1 6.03 us: expert_half(): outgoing = padded[owners].reshape(experts, capacity, normed.shape[1])]
    reduce_scatter x0 -> x1, waiting for transfers between devices: none -> 9.4 us  [dense_expert_half(): total = lax.psum_scatter(routed, 'ep', scatter_dimension=0, tiled=True)]
    dot_general x8 -> x7, matrix products: 24.4 us -> 21.8 us  [the longest x1 5.35 us: dense_expert_half(): jnp.dot(rows, routed_gate_weight[0], preferred_element_type=jnp.float32)]
  transfers between devices with their start and end apart: 5 -> 5, of which waited for: 4 -> 5; matrix products, arithmetic and copies ran while one was open for 22% -> 25% of each run, Pallas kernels for 0% -> 0%
where the time goes in v1:
time: 199 us; the launch traced here: 198 us
  waiting for transfers between devices  98.3 us (49%)
  matrix products  29.8 us (15%)
  other arithmetic  28.2 us (14%)
  blocking collectives  19.1 us (10%)
  between operations  14.1 us (7%)
  local copies, waits for them, and re-layouts  8.28 us (4%)
    all_gather x1, waiting for transfers between devices, dense_expert_half(): everything = lax.all_gather(sent, 'ep', axis=0, tiled=True)  46.3 us
    all_gather x1, waiting for transfers between devices, carried_in(): lax.all_gather(part.astype(kind), axis)  22.4 us
    reduce_scatter x1, waiting for transfers between devices, mixer_half(): lax.psum_scatter(jnp.dot(gated_rows, recurrence_out_weight, preferred_ele...  13 us
    all_gather x1, blocking collectives, carried_in(): lax.all_gather(part.astype(kind), axis)  12.8 us
    select_n x8, other arithmetic, turn(): return jax.tree.map(lambda a, b: jnp.where(reached, a, b), new, before)  10.4 us
    reduce_scatter x1, waiting for transfers between devices, dense_expert_half(): total = lax.psum_scatter(routed, 'ep', scatter_dimension=0, tiled=True)  9.4 us
    all_gather x1, waiting for transfers between devices, dense_expert_half(): hidden_full = lax.all_gather(hidden, 'tp', axis=1, tiled=True)  7.09 us
    all_gather x1, blocking collectives, dense_expert_half(): shared_full = lax.all_gather(shared_hidden, 'tp', axis=1, tiled=True)  6.33 us
  transfers between devices with their start and end apart: 5, of which 5 were waited for; matrix products, arithmetic and copies ran while one was open for 25% of the time, Pallas kernels for 0%

profile of v1, /device:TPU:0, one launch (start us, length us, event | category | flops | bytes accessed | tf_op | source)
XLA Modules:
  0.0 198.3 jit_solution(6184943672864648955)
XLA Ops:
  7.3 1.4 fusion.22
  16.9 1.9 fusion.38
  18.8 46.3 %all-gather.6.cloned.1.call-done = bf16[1024,2176]{1,0:T(8,128)(2,1)} async-done(((bf16[128,2176]{1,0:T(8,128)(2,1)}), bf16[1024,2176]{1,0:T(8,128)(2,1)}) %all-gather.6.cloned.1.call-update) | async-done | bytes 4456464 | tf_op jit(solution)/shard_map/all_gather | solution.py:221
  66.5 5.3 %fusion.3 = f32[1024,512]{1,0:T(8,128)S(1)} fusion(bf16[1024,2176]{1,0:T(8,128)(2,1)} %all-gather.6.cloned.1.call-done, bf16[1,2048,512]{2,1,0:T(8,128)(2,1)} %param.34), kind=kOutput, calls=%fused_computation.8 | convolution fusion | flops 2147483648 | bytes 8388608 | tf_op jit(solution)/shard_map/dot_general | solution.py:230
  71.9 3.6 %multiply_convert_fusion = bf16[1024,512]{1,0:T(8,128)(2,1)} fusion(f32[1024,512]{1,0:T(8,128)S(1)} %fusion.3, bf16[1,2048,512]{2,1,0:T(8,128)(2,1)S(1)} %copy-done.8, bf16[1024,2176]{1,0:T(8,128)(2,1)S(1)} %bitcast.139, f32[1024]{0:T(1024)S(1)} %fusion.37), kind=kOutput, calls=%fused_computation.15 | convolution fusion | flops 2151153664 | bytes 9441280 | tf_op jit(solution)/shard_map/dot_general | solution.py:231
  77.0 2.5 %bitcast_multiply_fusion.1 = (bf16[8,2,64,128]{3,0,1,2:T(8,128)(2,1)S(1)}, bf16[8,2,64,128]{3,0,1,2:T(8,128)(2,1)}, bf16[8,2,64,128]{3,0,1,2:T(8,128)(2,1)}, bf16[8,2,64,128]{3,0,1,2:T(8,128)(2,1)}) fusion(f32[8,2,64,128]{3,0,1,2:T(8,128)} %fusion.38, f32[8,2,128]{2,0,1:T(8,128)S(1)} %get-tuple-element.192, f32[8,2,128]{2,0,1:T(8,128)S(1)} %get-tuple-element.193, ...), kind=kLoop, calls=%fused_computation.54 | loop fusion | flops 1441792 | bytes 2637824 | tf_op jit(solution)/shard_map/mul | solution.py:84
  79.5 1.3 fusion.41
  80.8 4.5 %while.27 = (s32[]{:T(128)}, f32[8,128,128]{2,1,0:T(8,128)S(1)}, f32[2,8,128,128]{3,2,1,0:T(8,128)}, f32[2,8,128]{2,1,0:T(8,128)S(1)}, f32[2,8,128,128]{3,2,1,0:T(8,128)}, /*index=5*/s32[]{:T(128)}, s32[]{:T(128)}) while((s32[]{:T(128)}, f32[8,128,128]{2,1,0:T(8,128)S(1)}, f32[2,8,128,128]{3,2,1,0:T(8,128)}, ...), condition=%wide.region_2.3_spmd.clone, body=%wide.region_1.2_spmd.clone.sunk | while | flops 524291 | bytes 2633836 | solution.py:96
  81.7 1.4 bitcast_add_fusion.3
  83.9 1.4 bitcast_add_fusion.3
  86.2 12.8 %all-gather = bf16[64,128]{1,0:T(8,128)(2,1)S(1)} all-gather(bf16[8,128]{1,0:T(8,128)(2,1)S(1)} %exponential_convert_fusion), channel_id=2, replica_groups=mesh['grp'=2,'ep'=8,'tp'=2] {'ep'}, dimensions={0}, use_global_device_ids=true | all-gather | bytes 18432 | tf_op jit(solution)/shard_map/all_gather | solution.py:18
  100.5 7.1 %all-gather.8.cloned.1.call-done = bf16[1024,1024]{1,0:T(8,128)(2,1)} async-done(((bf16[1024,512]{1,0:T(8,128)(2,1)}), bf16[1024,1024]{1,0:T(8,128)(2,1)}) %all-gather.8.cloned.1.call-update) | async-done | bytes 2097168 | tf_op jit(solution)/shard_map/all_gather | solution.py:234
  107.6 5.2 %fusion.9 = bf16[1024,1024]{1,0:T(8,128)(2,1)} fusion(bf16[1024,1024]{1,0:T(8,128)(2,1)} %all-gather.8.cloned.1.call-done, bf16[1,1024,1024]{2,1,0:T(8,128)(2,1)S(1)} %copy-done), kind=kOutput, calls=%fused_computation.16 | convolution fusion | flops 2148532224 | bytes 6291456 | tf_op jit(solution)/shard_map/dot_general | solution.py:236
  113.7 2.2 %fusion.17 = f32[8,2,64,128]{3,2,1,0:T(8,128)} fusion(bf16[8,2,64,128]{3,0,1,2:T(8,128)(2,1)S(1)} %copy-done.4, bf16[8,2,64,128]{3,0,1,2:T(8,128)(2,1)} %get-tuple-element.189, bf16[8,2,64,128]{3,0,2,1:T(8,128)(2,1)} %bitcast_bitcast_fusion, pred[64,64]{1,0:T(8,128)(4,1)S(1)} %iota_compare_fusion.1), kind=kOutput, calls=%fused_computation.22 | convolution fusion | flops 33619968 | bytes 1314816 | tf_op jit(solution)/shard_map/hncs,hnse->hnce/dot_general | solution.py:81
  115.9 22.4 %all-gather.10.cloned.1.call-done = bf16[64,128,128]{2,1,0:T(8,128)(2,1)} async-done(((bf16[8,128,128]{2,1,0:T(8,128)(2,1)}), bf16[64,128,128]{2,1,0:T(8,128)(2,1)}) %all-gather.10.cloned.1.call-update) | async-done | bytes 2097168 | tf_op jit(solution)/shard_map/all_gather | solution.py:18
  138.3 10.8 %while.28 = (s32[]{:T(128)}, f32[8,128,128]{2,1,0:T(8,128)S(1)}, s32[]{:T(128)}, bf16[8,8,128]{2,1,0:T(8,128)(2,1)S(1)}, bf16[8,8,128,128]{3,2,1,0:T(8,128)(2,1)}, /*index=5*/s32[]{:T(128)}, s32[]{:T(128)}) while((s32[]{:T(128)}, f32[8,128,128]{2,1,0:T(8,128)S(1)}, s32[]{:T(128)}, bf16[8,8,128]{2,1,0:T(8,128)(2,1)S(1)}, ...), condition=%wide.region_6.7_spmd.clone, body=%wide.region_5.6_spmd.clone.sunk | while | flops 656388 | bytes 1321073 | solution.py:35
  138.3 1.3 fusion.73
  139.7 1.3 fusion.73
  141.1 1.3 fusion.73
  142.4 1.3 fusion.73
  143.8 1.3 fusion.73
  145.1 1.3 fusion.73
  146.5 1.3 fusion.73
  147.8 1.3 fusion.73
  149.2 2.7 %multiply_reduce_fusion = (f32[2,64,8]{1,0,2:T(2,128)S(1)}, f32[2,64,8,128]{3,1,0,2:T(8,128)}) fusion(f32[8,2,64,128]{3,2,1,0:T(8,128)} %fusion.17, bf16[8,2,64,128]{3,0,1,2:T(8,128)(2,1)S(1)} %copy-done.1, f32[2,8,128,128]{3,2,1,0:T(8,128)} %get-tuple-element.124, f32[8,128,128]{2,1,0:T(8,128)S(1)} %get-tuple-element.126, f32[2,8,128]{2,1,0:T(8,128)S(1)} %fusion.21), kind=kOutput, calls=%fused_computation.66 | convolution fusion | flops 34733056 | bytes 2895872 | tf_op jit(solution)/shard_map/hncd,nhde->hnce/dot_general | solution.py:102
  151.9 1.4 copy.67
  153.5 4.0 %convolution_convert_fusion = bf16[128,2048]{1,0:T(8,128)(2,1)} fusion(bf16[1024,2048]{1,0:T(8,128)(2,1)} %param.29, bf16[128,1024]{1,0:T(8,128)(2,1)} %param.25, f32[16,8,8,128]{3,2,1,0:T(8,128)S(1)} %bitcast.133, f32[16,8,8,128]{3,2,1,0:T(8,128)S(1)} %bitcast.134, f32[1024]{0:T(1024)S(1)} %copy-done.10), kind=kOutput, calls=%fused_computation.10 | convolution fusion | flops 538312704 | bytes 6033408 | tf_op jit(solution)/shard_map/dot_general | solution.py:112
  157.6 2.2 %fusion.60 = f32[128,512]{1,0:T(8,128)S(1)} fusion(bf16[128,2048]{1,0:T(8,128)(2,1)S(1)} %fusion.24, bf16[2048,512]{1,0:T(8,128)(2,1)} %param.37), kind=kOutput, calls=%fused_computation.94 | convolution fusion | flops 268435456 | bytes 2883584 | tf_op jit(solution)/shard_map/dot_general | solution.py:227
  160.3 6.3 %all_gather.22 = bf16[128,1024]{1,0:T(8,128)(2,1)S(1)} all-gather(bf16[128,512]{1,0:T(8,128)(2,1)S(1)} %fusion.19), channel_id=1, replica_groups=mesh['grp'=2,'ep'=8,'tp'=2] {'tp'}, dimensions={1}, use_global_device_ids=true | all-gather | bytes 393216 | tf_op jit(solution)/shard_map/all_gather | solution.py:233
  166.6 9.4 %reduce-scatter.5.cloned.1.call-done = bf16[128,1024]{1,0:T(8,128)(2,1)} async-done(((bf16[1024,1024]{1,0:T(8,128)(2,1)}), bf16[128,1024]{1,0:T(8,128)(2,1)}) %reduce-scatter.5.cloned.1.call-update) | async-done | bytes 262160 | tf_op jit(solution)/shard_map/reduce_scatter | solution.py:239
  176.0 2.7 %fusion.18 = bf16[128,1024]{1,0:T(8,128)(2,1)} fusion(bf16[128,1024]{1,0:T(8,128)(2,1)S(1)} %all_gather.22, bf16[1024,1024]{1,0:T(8,128)(2,1)} %param.39, bf16[128,1024]{1,0:T(8,128)(2,1)} %reduce-scatter.5.cloned.1.call-done), kind=kOutput, calls=%fused_computation.24 | convolution fusion | flops 268828672 | bytes 2883584 | tf_op jit(solution)/shard_map/dot_general | solution.py:235
  178.7 13.0 %reduce-scatter.3.cloned.1.call-done = bf16[64,2048]{1,0:T(8,128)(2,1)} async-done(((bf16[128,2048]{1,0:T(8,128)(2,1)}), bf16[64,2048]{1,0:T(8,128)(2,1)}) %reduce-scatter.3.cloned.1.call-update) | async-done | bytes 262160 | tf_op jit(solution)/shard_map/reduce_scatter | solution.py:111
  (83 shorter events, 16.9 us)
Async XLA Ops:
  7.2 100.4 %copy-start = (bf16[1,1024,1024]{2,1,0:T(8,128)(2,1)S(1)}, bf16[1,1024,1024]{2,1,0:T(8,128)(2,1)}, u32[]{:S(2)}) copy-start(bf16[1,1024,1024]{2,1,0:T(8,128)(2,1)} %param.36) | copy-start | bytes 6291460
  7.2 6.1 %copy-start.7 = (f32[128,8]{0,1:T(8,128)S(1)}, f32[128,8]{0,1:T(8,128)}, u32[]{:S(2)}) copy-start(f32[128,8]{0,1:T(8,128)} %param.27) | copy-start | bytes 12292
  7.2 6.4 %copy-start.2 = (bf16[128,1024]{1,0:T(8,128)(2,1)S(1)}, bf16[128,1024]{1,0:T(8,128)(2,1)}, u32[]{:S(2)}) copy-start(bf16[128,1024]{1,0:T(8,128)(2,1)} %param.23) | copy-start | bytes 786436
  7.2 6.4 %copy-start.6 = (f32[1024]{0:T(1024)S(1)}, f32[1024]{0:T(1024)}, u32[]{:S(2)}) copy-start(f32[1024]{0:T(1024)} %param.26) | copy-start | bytes 12292
  7.2 57.9 %all-gather.6.cloned.1.call-start = ((), (), s32[]{:S(2)}) async-start(), calls=%async_computation.3 | async-start | bytes 5013504 | tf_op jit(solution)/shard_map/all_gather | solution.py:221
  13.2 94.3 %all-gather.8.cloned.1.call-start = ((), (), s32[]{:S(2)}) async-start(), calls=%async_computation.4 | async-start | bytes 3145728 | tf_op jit(solution)/shard_map/all_gather | solution.py:234
  13.4 1.5 copy-start.3
  14.0 2.9 %copy-start.5 = (bf16[128,1024]{1,0:T(8,128)(2,1)S(1)}, bf16[128,1024]{1,0:T(8,128)(2,1)}, u32[]{:S(2)}) copy-start(bf16[128,1024]{1,0:T(8,128)(2,1)} %param.24) | copy-start | bytes 786436
  66.1 5.8 %slice-start = ((s8[4456448]{0:T(1024)(128)(4,1)}), s8[4194304]{0:T(1024)(128)(4,1)S(1)}, s32[]{:S(2)}) async-start(s8[4456448]{0:T(1024)(128)(4,1)} %bitcast.138), calls=%async_computation.7 | async-start | bytes 8388608
  66.5 5.4 %slice-start.1 = ((s8[4456448]{0:T(1024)(128)(4,1)}), s8[262144]{0:T(1024)(128)(4,1)S(1)}, s32[]{:S(2)}) async-start(s8[4456448]{0:T(1024)(128)(4,1)} %bitcast.138), calls=%async_computation.8 | async-start | bytes 524288
  66.5 5.4 %copy-start.8 = (bf16[1,2048,512]{2,1,0:T(8,128)(2,1)S(1)}, bf16[1,2048,512]{2,1,0:T(8,128)(2,1)}, u32[]{:S(2)}) copy-start(bf16[1,2048,512]{2,1,0:T(8,128)(2,1)} %param.35) | copy-start | bytes 6291460
  75.5 62.8 %all-gather.10.cloned.1.call-start = ((), (), s32[]{:S(2)}) async-start(), calls=%async_computation.6 | async-start | bytes 2359296 | tf_op jit(solution)/shard_map/all_gather | solution.py:18
  86.1 89.9 %reduce-scatter.5.cloned.1.call-start = ((), (), s32[]{:S(2)}) async-start(), calls=%async_computation.5 | async-start | bytes 2359296 | tf_op jit(solution)/shard_map/reduce_scatter | solution.py:239
  112.8 0.9 copy-start.4
  112.8 79.0 %reduce-scatter.3.cloned.1.call-start = ((), (), s32[]{:S(2)}) async-start(), calls=%async_computation.2 | async-start | bytes 786432 | tf_op jit(solution)/shard_map/reduce_scatter | solution.py:111
  138.3 10.8 %copy-start.1 = (bf16[8,2,64,128]{3,0,1,2:T(8,128)(2,1)S(1)}, bf16[8,2,64,128]{3,0,1,2:T(8,128)(2,1)}, u32[]{:S(2)}) copy-start(bf16[8,2,64,128]{3,0,1,2:T(8,128)(2,1)} %get-tuple-element.190) | copy-start | bytes 786436
  149.1 4.3 %copy-start.10 = (f32[1024]{0:T(1024)S(1)}, f32[1024]{0:T(1024)}, u32[]{:S(2)}) copy-start(f32[1024]{0:T(1024)} %param.28) | copy-start | bytes 12292
  157.5 2.3 %copy-start.9 = (bf16[2048,512]{1,0:T(8,128)(2,1)S(1)}, bf16[2048,512]{1,0:T(8,128)(2,1)}, u32[]{:S(2)}) copy-start(bf16[2048,512]{1,0:T(8,128)(2,1)} %param.38) | copy-start | bytes 6291460
Sparse Core Ops, SparseCore 0:
  13.4 51.7 all-gather.5
  75.6 31.8 all-gather.7
  109.2 29.1 all-gather.9
  140.5 35.4 reduce-scatter.4
  178.7 13.0 reduce-scatter.2

commit v2 on v1

--- a/solution.py
+++ b/solution.py
@@ -1,6 +1,10 @@
+import functools
+
 import jax
 import jax.numpy as jnp
 from jax import lax
+from jax.experimental import pallas as pl
+from jax.experimental.pallas import tpu as pltpu
 from jax.sharding import PartitionSpec as P
 
 HEAD_CHANNELS = 128
@@ -191,6 +195,216 @@
     return combined.astype(jnp.bfloat16)
 
 
+MESH = pl.DeviceIdType.MESH
+LANES = 128
+
+
+def expert_kernel(
+    count,
+    x_ref,
+    gate_hbm,
+    up_hbm,
+    down_hbm,
+    shared_gate_hbm,
+    shared_up_hbm,
+    shared_down_hbm,
+    routed_ref,
+    shared_ref,
+    rows,
+    gate_w,
+    up_w,
+    down_w,
+    shared_gate_w,
+    shared_up_w,
+    shared_down_w,
+    own_hidden,
+    peer_hidden,
+    load_sem,
+    right_sem,
+    left_sem,
+    side_sem,
+    row_sem,
+    hidden_send,
+    hidden_recv,
+):
+    chips = count // 2
+    me = lax.axis_index("ep")
+    half = lax.axis_index("tp")
+    chip, core = me // 2, me % 2
+    side = chip * 2 + 1 - core
+    partner = 1 - half
+    block_rows = x_ref.shape[0]
+    width = gate_w.shape[0]
+    units = gate_w.shape[1]
+    has_right, has_left = chip < chips - 1, chip > 0
+
+    def half_rows(ref, which):
+        return ref.at[pl.ds(pl.multiple_of(which * units, units), units), :]
+
+    loads = [
+        (shared_gate_hbm, shared_gate_w),
+        (shared_up_hbm, shared_up_w),
+        (gate_hbm.at[0], gate_w),
+        (up_hbm.at[0], up_w),
+        (half_rows(down_hbm.at[0], half), down_w.at[0]),
+        (half_rows(down_hbm.at[0], partner), down_w.at[1]),
+        (half_rows(shared_down_hbm, half), shared_down_w.at[0]),
+        (half_rows(shared_down_hbm, partner), shared_down_w.at[1]),
+        (x_ref, rows.at[me]),
+    ]
+    copies = [
+        pltpu.make_async_copy(source, target, load_sem.at[i])
+        for i, (source, target) in enumerate(loads)
+    ]
+    for copy in copies:
+        copy.start()
+
+    barrier = pltpu.get_barrier_semaphore()
+    pl.semaphore_signal(barrier, inc=1, device_id={"ep": side}, device_id_type=MESH)
+    pl.semaphore_signal(barrier, inc=1, device_id={"tp": partner}, device_id_type=MESH)
+
+    @pl.when(has_right)
+    def _():
+        pl.semaphore_signal(barrier, inc=1, device_id={"ep": me + 2}, device_id_type=MESH)
+
+    @pl.when(has_left)
+    def _():
+        pl.semaphore_signal(barrier, inc=1, device_id={"ep": me - 2}, device_id_type=MESH)
+
+    pl.semaphore_wait(barrier, 2 + has_right.astype(jnp.int32) + has_left.astype(jnp.int32))
+
+    def row_copy(source, block, sems, target):
+        return pltpu.make_async_remote_copy(
+            src_ref=source,
+            dst_ref=rows.at[block],
+            send_sem=sems.at[block],
+            recv_sem=row_sem.at[block],
+            device_id={"ep": target},
+            device_id_type=MESH,
+        )
+
+    def hidden_copy(step):
+        return pltpu.make_async_remote_copy(
+            src_ref=own_hidden.at[step],
+            dst_ref=peer_hidden.at[step],
+            send_sem=hidden_send.at[step],
+            recv_sem=hidden_recv.at[step],
+            device_id={"tp": partner},
+            device_id_type=MESH,
+        )
+
+    def block_of(step):
+        k, odd = step // 2, step % 2
+        inner = jnp.minimum(chip, chips - 1 - chip)
+        near = jnp.where(k % 2 == 1, chip - (k + 1) // 2, chip + k // 2)
+        far = jnp.where(chip <= chips - 1 - chip, k, chips - 1 - k)
+        source = jnp.where(k <= 2 * inner, near, far)
+        return source, source * 2 + jnp.where(odd == 1, 1 - core, core)
+
+    def goes_right(source):
+        return jnp.logical_and(source <= chip, has_right)
+
+    def goes_left(source):
+        return jnp.logical_and(source >= chip, has_left)
+
+    @pl.when(has_right)
+    def _():
+        row_copy(x_ref, me, right_sem, me + 2).start()
+
+    @pl.when(has_left)
+    def _():
+        row_copy(x_ref, me, left_sem, me - 2).start()
+
+    row_copy(x_ref, me, side_sem, side).start()
+
+    copies[0].wait()
+    copies[1].wait()
+    gate_part = jnp.dot(
+        x_ref[:, :width], shared_gate_w[...], preferred_element_type=jnp.float32
+    )
+    up_part = jnp.dot(x_ref[:, :width], shared_up_w[...], preferred_element_type=jnp.float32)
+    own_hidden[count] = (jax.nn.silu(gate_part) * up_part).astype(jnp.bfloat16)
+    for copy in copies[2:]:
+        copy.wait()
+
+    def down(step, weight):
+        hidden_copy(step).wait_recv()
+        return jnp.dot(
+            own_hidden[step], weight[0], preferred_element_type=jnp.float32
+        ) + jnp.dot(peer_hidden[step], weight[1], preferred_element_type=jnp.float32)
+
+    def routed_down(step):
+        _, block = block_of(step)
+        place = pl.ds(pl.multiple_of(block * block_rows, block_rows), block_rows)
+        routed_ref[place, :] = down(step, down_w).astype(jnp.bfloat16)
+
+    def turn(step, _):
+        source, block = block_of(step)
+        odd = step % 2
+
+        @pl.when(step > 0)
+        def _():
+            row_copy(x_ref, block, side_sem, side).wait_recv()
+
+        @pl.when(jnp.logical_and(step > 0, odd == 0))
+        def _():
+            @pl.when(goes_right(source))
+            def _():
+                row_copy(rows.at[block], block, right_sem, me + 2).start()
+
+            @pl.when(goes_left(source))
+            def _():
+                row_copy(rows.at[block], block, left_sem, me - 2).start()
+
+            row_copy(rows.at[block], block, side_sem, side).start()
+
+        x = rows[block, :, :width]
+        tail = rows[block, :, width:].astype(jnp.float32)
+        lane = lax.broadcasted_iota(jnp.int32, tail.shape, 1)
+        own_gate = jnp.sum(
+            jnp.where(lane % (LANES // 2) == me, tail, 0.0), axis=1, keepdims=True
+        )
+        gate_part = jnp.dot(x, gate_w[...], preferred_element_type=jnp.float32)
+        up_part = jnp.dot(x, up_w[...], preferred_element_type=jnp.float32)
+        own_hidden[step] = (jax.nn.silu(gate_part) * up_part * own_gate).astype(jnp.bfloat16)
+
+        @pl.when(step == 0)
+        def _():
+            hidden_copy(count).start()
+
+        @pl.when(step > 0)
+        def _():
+            routed_down(step - 1)
+
+        hidden_copy(step).start()
+        return 0
+
+    lax.fori_loop(0, count, turn, 0)
+    shared_ref[...] = down(count, shared_down_w)
+    routed_down(count - 1)
+
+    def finish(step, _):
+        source, block = block_of(step)
+        hidden_copy(step).wait_send()
+
+        @pl.when(step % 2 == 0)
+        def _():
+            @pl.when(goes_right(source))
+            def _():
+                row_copy(x_ref, block, right_sem, me + 2).wait_send()
+
+            @pl.when(goes_left(source))
+            def _():
+                row_copy(x_ref, block, left_sem, me - 2).wait_send()
+
+            row_copy(x_ref, block, side_sem, side).wait_send()
+
+        return 0
+
+    lax.fori_loop(0, count, finish, 0)
+    hidden_copy(count).wait_send()
+
+
 def dense_expert_half(
     expert_hidden_state,
     chosen_expert_index,
@@ -203,39 +417,71 @@
     shared_up_weight,
     shared_down_weight,
 ):
-    tokens, top = chosen_expert_index.shape
-    experts = lax.axis_size("ep")
+    tokens = chosen_expert_index.shape[0]
+    count = lax.axis_size("ep")
     features = expert_hidden_state.astype(jnp.float32)
     width = features.shape[1]
+    units, width_out = routed_gate_weight.shape[2], routed_down_weight.shape[2]
     normed = (
         features
         * lax.rsqrt(jnp.mean(features * features, axis=1, keepdims=True) + EPSILON)
         * expert_norm_gain[None, :]
     ).astype(jnp.bfloat16)
     gates = ROUTED_SCALE * chosen_expert_score / jnp.sum(chosen_expert_score, axis=1, keepdims=True)
-    chosen = chosen_expert_index[:, :, None] == jnp.arange(64, dtype=jnp.int32)[None, None, :]
+    slots = LANES // 2
+    chosen = chosen_expert_index[:, :, None] == jnp.arange(slots, dtype=jnp.int32)[None, None, :]
     gate_table = jnp.sum(jnp.where(chosen, gates[:, :, None], 0.0), axis=1)
     high = gate_table.astype(jnp.bfloat16)
     low = (gate_table - high.astype(jnp.float32)).astype(jnp.bfloat16)
     sent = jnp.concatenate([normed, high, low], axis=1)
-    everything = lax.all_gather(sent, "ep", axis=0, tiled=True)
-    rows = everything[:, :width]
-    mine = jnp.arange(64, dtype=jnp.int32) == lax.axis_index("ep")
-    tail = everything[:, width:].astype(jnp.float32)
-    own_gate = jnp.sum(jnp.where(mine[None, :], tail[:, :64] + tail[:, 64:], 0.0), axis=1)
-    shared_hidden = (
-        jax.nn.silu(jnp.dot(normed, shared_gate_weight, preferred_element_type=jnp.float32))
-        * jnp.dot(normed, shared_up_weight, preferred_element_type=jnp.float32)
-    ).astype(jnp.bfloat16)
-    gate_part = jnp.dot(rows, routed_gate_weight[0], preferred_element_type=jnp.float32)
-    up_part = jnp.dot(rows, routed_up_weight[0], preferred_element_type=jnp.float32)
-    hidden = (jax.nn.silu(gate_part) * up_part * own_gate[:, None]).astype(jnp.bfloat16)
-    shared_full = lax.all_gather(shared_hidden, "tp", axis=1, tiled=True)
-    hidden_full = lax.all_gather(hidden, "tp", axis=1, tiled=True)
-    shared = jnp.dot(shared_full, shared_down_weight, preferred_element_type=jnp.float32)
-    routed = jnp.dot(
-        hidden_full, routed_down_weight[0], preferred_element_type=jnp.float32
-    ).astype(jnp.bfloat16)
+    hbm = pl.BlockSpec(memory_space=pl.ANY)
+    vmem = pl.BlockSpec(memory_space=pltpu.VMEM)
+    weight = pltpu.VMEM((width, units), jnp.bfloat16)
+    down_weight = pltpu.VMEM((2, units, width_out), jnp.bfloat16)
+    hidden = pltpu.VMEM((count + 1, tokens, units), jnp.bfloat16)
+    block_sems = pltpu.SemaphoreType.DMA((count,))
+    routed, shared = pl.pallas_call(
+        functools.partial(expert_kernel, count),
+        out_shape=(
+            jax.ShapeDtypeStruct((count * tokens, width_out), jnp.bfloat16),
+            jax.ShapeDtypeStruct((tokens, width_out), jnp.float32),
+        ),
+        in_specs=[vmem] + [hbm] * 6,
+        out_specs=(vmem, vmem),
+        scratch_shapes=[
+            pltpu.VMEM((count, tokens, width + LANES), jnp.bfloat16),
+            weight,
+            weight,
+            down_weight,
+            weight,
+            weight,
+            down_weight,
+            hidden,
+            hidden,
+            pltpu.SemaphoreType.DMA((9,)),
+            block_sems,
+            block_sems,
+            block_sems,
+            block_sems,
+            pltpu.SemaphoreType.DMA((count + 1,)),
+            pltpu.SemaphoreType.DMA((count + 1,)),
+        ],
+        compiler_params=pltpu.CompilerParams(
+            collective_id=0, has_side_effects=True, vmem_limit_bytes=48 * 1024 * 1024
+        ),
+        cost_estimate=pl.CostEstimate(
+            flops=45_000_000_000, bytes_accessed=16_000_000, transcendentals=0
+        ),
+        name="expert_kernel",
+    )(
+        sent,
+        routed_gate_weight,
+        routed_up_weight,
+        routed_down_weight,
+        shared_gate_weight,
+        shared_up_weight,
+        shared_down_weight,
+    )
     total = lax.psum_scatter(routed, "ep", scatter_dimension=0, tiled=True)
     return (shared + total.astype(jnp.float32)).astype(jnp.bfloat16)
 

time: 199 us -> 147 us (0.74)
  waiting for transfers between devices: 98.3 us -> 19.2 us
  Pallas kernels: 0 us -> 72.1 us
  matrix products: 29.8 us -> 5.7 us
  other arithmetic: 28.2 us -> 19.3 us
  blocking collectives: 19.1 us -> 12.8 us
  local copies, waits for them, and re-layouts: 8.28 us -> 2.83 us
    pallas_call x0 -> x1, Pallas kernels: none -> 72.1 us  [dense_expert_half(): pl.pallas_call(functools.partial(expert_kernel, count), out_shape=(jax.Sh...]
    all_gather x2 -> x0, waiting for transfers between devices: 53.4 us -> none  [the longest x1 46.3 us: dense_expert_half(): everything = lax.all_gather(sent, 'ep', axis=0, tiled=True)]
    all_gather x1, waiting for transfers between devices: 22.4 us -> 0.02 us  [carried_in(): lax.all_gather(part.astype(kind), axis)]
    dot_general x6 -> x0, matrix products: 19.5 us -> none  [the longest x1 5.35 us: dense_expert_half(): jnp.dot(rows, routed_gate_weight[0], preferred_element_type=jnp.float32)]
    all_gather x1 -> x0, blocking collectives: 6.33 us -> none  [dense_expert_half(): shared_full = lax.all_gather(shared_hidden, 'tp', axis=1, tiled=True)]
    reduce_scatter x1, waiting for transfers between devices: 9.4 us -> 4.72 us  [dense_expert_half(): total = lax.psum_scatter(routed, 'ep', scatter_dimension=0, tiled=True)]
    unnamed x31, local copies, waits for them, and re-layouts: 3.83 us -> 1.54 us
    add x2, other arithmetic: 2.72 us -> 0.58 us  [advance(): return (factor[..., None] * carry_state + update, carry_state)]
  transfers between devices with their start and end apart: 5 -> 3, of which waited for: 5 -> 2; matrix products, arithmetic and copies ran while one was open for 25% -> 14% of each run, Pallas kernels for 0% -> 49%
where the time goes in v2:
time: 147 us
  Pallas kernels  72.1 us (49%)
  other arithmetic  19.3 us (13%)
  waiting for transfers between devices  19.2 us (13%)
  between operations  14.2 us (10%)
  blocking collectives  12.8 us (9%)
  matrix products  5.7 us (4%)
  local copies, waits for them, and re-layouts  2.83 us (2%)
    pallas_call x1, Pallas kernels, dense_expert_half(): pl.pallas_call(functools.partial(expert_kernel, count), out_shape=(jax.Sh...  72.1 us
    reduce_scatter x1, waiting for transfers between devices, mixer_half(): lax.psum_scatter(jnp.dot(gated_rows, recurrence_out_weight, preferred_ele...  14.4 us
    all_gather x1, blocking collectives, carried_in(): lax.all_gather(part.astype(kind), axis)  12.8 us
    select_n x8, other arithmetic, turn(): return jax.tree.map(lambda a, b: jnp.where(reached, a, b), new, before)  10.5 us
    reduce_scatter x1, waiting for transfers between devices, dense_expert_half(): total = lax.psum_scatter(routed, 'ep', scatter_dimension=0, tiled=True)  4.72 us
    dot_general x1, matrix products, mixer_half(): jnp.dot(gated_rows, recurrence_out_weight, preferred_element_type=jnp.flo...  4.02 us
  transfers between devices with their start and end apart: 3, of which 2 were waited for; matrix products, arithmetic and copies ran while one was open for 14% of the time, Pallas kernels for 49%

profile of v2, /device:TPU:0, one launch (start us, length us, event | category | flops | bytes accessed | tf_op | source)
XLA Modules:
  0.0 146.6 jit_solution(12428046526951332175)
XLA Ops:
  7.2 0.8 copy.72
  8.2 1.3 fusion.38
  10.2 0.3 copy-done.8
  10.6 1.1 bitcast_multiply_fusion.1
  11.8 0.3 fusion.22
  12.2 2.3 %while.27 = (s32[]{:T(128)}, f32[8,128,128]{2,1,0:T(8,128)S(1)}, f32[2,8,128,128]{3,2,1,0:T(8,128)}, f32[2,8,128]{2,1,0:T(8,128)S(1)}, f32[2,8,128,128]{3,2,1,0:T(8,128)S(1)}, /*index=5*/s32[]{:T(128)}, s32[]{:T(128)}) while((s32[]{:T(128)}, f32[8,128,128]{2,1,0:T(8,128)S(1)}, f32[2,8,128,128]{3,2,1,0:T(8,128)}, ...), condition=%wide.region_2.3_spmd.clone, body=%wide.region_1.2_spmd.clone.sunk | while | flops 524291 | bytes 2634336 | solution.py:100
  12.2 0.8 bitcast_dynamic-update-slice_fusion.2
  13.0 0.3 bitcast_add_fusion.3
  13.3 0.9 bitcast_dynamic-update-slice_fusion.2
  14.2 0.3 bitcast_add_fusion.3
  14.5 0.8 convert_element_type.81
  16.1 0.3 concatenate.3.x_ref
  16.4 72.1 %expert_kernel.1 = (bf16[1024,1024]{1,0:T(8,128)(2,1)}, f32[128,1024]{1,0:T(8,128)S(1)}) custom-call(bf16[128,2176]{1,0:T(8,128)(2,1)S(1)} %concatenate.3.x_ref, bf16[1,2048,512]{2,1,0:T(8,128)(2,1)S(1)} %copy-done, bf16[1,2048,512]{2,1,0:T(8,128)(2,1)} %up_hbm.1, bf16[1,1024,1024]{2,1,0:T(8,128)(2,1)} %down_hbm.1, bf16[2048,512]{1,0:T(8,128)(2,1)} %shared_gate_hbm.1, ...), custom_call_target="tpu_custom_call" | custom-call | flops 44999999488 | bytes 16000000 | tf_op jit(solution)/shard_map/expert_kernel/pallas_call | solution.py:443
  88.6 0.8 fusion.4
  89.5 12.8 %all-gather = bf16[64,128]{1,0:T(8,128)(2,1)S(1)} all-gather(bf16[8,128]{1,0:T(8,128)(2,1)S(1)} %exponential_convert_fusion), channel_id=2, replica_groups=mesh['grp'=2,'ep'=8,'tp'=2] {'ep'}, dimensions={0}, use_global_device_ids=true | all-gather | bytes 18432 | tf_op jit(solution)/shard_map/all_gather | solution.py:22
  102.3 0.4 fusion.2
  102.7 10.8 %while.28 = (s32[]{:T(128)}, f32[8,128,128]{2,1,0:T(8,128)S(1)}, s32[]{:T(128)}, bf16[8,8,128]{2,1,0:T(8,128)(2,1)S(1)}, bf16[8,8,128,128]{3,2,1,0:T(8,128)(2,1)}, /*index=5*/s32[]{:T(128)}, s32[]{:T(128)}) while((s32[]{:T(128)}, f32[8,128,128]{2,1,0:T(8,128)S(1)}, s32[]{:T(128)}, bf16[8,8,128]{2,1,0:T(8,128)(2,1)S(1)}, ...), condition=%wide.region_6.7_spmd.clone, body=%wide.region_5.6_spmd.clone.sunk | while | flops 656388 | bytes 1321065 | solution.py:39
  102.8 1.4 fusion.46
  104.2 1.3 fusion.46
  105.5 1.3 fusion.46
  106.9 1.3 fusion.46
  108.2 1.3 fusion.46
  109.6 1.3 fusion.46
  110.9 1.3 fusion.46
  112.3 1.3 fusion.46
  113.6 0.9 multiply_reduce_fusion
  114.7 0.3 copy.82
  115.0 0.2 mul.134
  115.2 4.0 %convolution_convert_fusion = bf16[128,2048]{1,0:T(8,128)(2,1)} fusion(bf16[1024,2048]{1,0:T(8,128)(2,1)} %param.29, bf16[128,1024]{1,0:T(8,128)(2,1)} %param.25, f32[16,8,8,128]{3,2,1,0:T(8,128)S(1)} %bitcast.113, f32[16,8,8,128]{3,2,1,0:T(8,128)S(1)} %bitcast.114, f32[1024]{0:T(1024)S(1)} %copy-done.12), kind=kOutput, calls=%fused_computation.6 | convolution fusion | flops 538312704 | bytes 6033408 | tf_op jit(solution)/shard_map/dot_general | solution.py:116
  119.2 4.7 %reduce-scatter.5.cloned.1.call-done = bf16[128,1024]{1,0:T(8,128)(2,1)} async-done(((bf16[1024,1024]{1,0:T(8,128)(2,1)}), bf16[128,1024]{1,0:T(8,128)(2,1)}) %reduce-scatter.5.cloned.1.call-update) | async-done | bytes 262160 | tf_op jit(solution)/shard_map/reduce_scatter | solution.py:485
  124.0 1.7 %add_convert_fusion = bf16[128,1024]{1,0:T(8,128)(2,1)} fusion(f32[128,1024]{1,0:T(8,128)S(1)} %get-tuple-element.129, bf16[128,1024]{1,0:T(8,128)(2,1)} %reduce-scatter.5.cloned.1.call-done), kind=kLoop, calls=%fused_computation.49 | loop fusion | flops 393216 | bytes 1048576 | tf_op jit(solution)/shard_map/convert_element_type | solution.py:486
  125.7 14.4 %reduce-scatter.3.cloned.1.call-done = bf16[64,2048]{1,0:T(8,128)(2,1)} async-done(((bf16[128,2048]{1,0:T(8,128)(2,1)}), bf16[64,2048]{1,0:T(8,128)(2,1)}) %reduce-scatter.3.cloned.1.call-update) | async-done | bytes 262160 | tf_op jit(solution)/shard_map/reduce_scatter | solution.py:115
  (69 shorter events, 2.0 us)
Async XLA Ops:
  7.2 95.5 %all-gather.4.cloned.1.call-start = ((), (), s32[]{:S(2)}) async-start(), calls=%async_computation.4 | async-start | bytes 2359296 | tf_op jit(solution)/shard_map/all_gather | solution.py:22
  8.2 1.8 %copy-start.5 = (bf16[128,1024]{1,0:T(8,128)(2,1)S(1)}, bf16[128,1024]{1,0:T(8,128)(2,1)}, u32[]{:S(2)}) copy-start(bf16[128,1024]{1,0:T(8,128)(2,1)} %param.22) | copy-start | bytes 786436
  9.6 1.0 copy-start.8
  9.8 2.0 %copy-start.1 = (f32[8,2,64,128]{3,0,1,2:T(8,128)}, f32[8,2,64,128]{3,0,1,2:T(8,128)S(1)}, u32[]{:S(2)}) copy-start(f32[8,2,64,128]{3,0,1,2:T(8,128)S(1)} %fusion.19) | copy-start | bytes 1572868
  12.1 3.2 %copy-start.10 = (f32[128,4]{0,1:T(4,128)S(1)}, f32[128,4]{0,1:T(4,128)}, u32[]{:S(2)}) copy-start(f32[128,4]{0,1:T(4,128)} %param.32) | copy-start | bytes 6148
  12.1 3.3 %copy-start.11 = (s32[128,4]{0,1:T(4,128)S(1)}, s32[128,4]{0,1:T(4,128)}, u32[]{:S(2)}) copy-start(s32[128,4]{0,1:T(4,128)} %param.31) | copy-start | bytes 6148
  12.1 3.5 %copy-start.2 = (bf16[128,2048]{1,0:T(8,128)(2,1)S(1)}, bf16[128,2048]{1,0:T(8,128)(2,1)}, u32[]{:S(2)}) copy-start(bf16[128,2048]{1,0:T(8,128)(2,1)} %param.30) | copy-start | bytes 1572868
  12.2 3.7 %copy-start.9 = (f32[2048]{0:T(1024)S(1)}, f32[2048]{0:T(1024)}, u32[]{:S(2)}) copy-start(f32[2048]{0:T(1024)} %param.33) | copy-start | bytes 24580
  14.5 1.9 %copy-start = (bf16[1,2048,512]{2,1,0:T(8,128)(2,1)S(1)}, bf16[1,2048,512]{2,1,0:T(8,128)(2,1)}, u32[]{:S(2)}) copy-start(bf16[1,2048,512]{2,1,0:T(8,128)(2,1)} %gate_hbm.1) | copy-start | bytes 6291460
  15.3 108.7 %reduce-scatter.5.cloned.1.call-start = ((), (), s32[]{:S(2)}) async-start(), calls=%async_computation.3 | async-start | bytes 2359296 | tf_op jit(solution)/shard_map/reduce_scatter | solution.py:485
  88.5 13.8 %copy-start.6 = (bf16[8,2,64,128]{3,0,1,2:T(8,128)(2,1)S(1)}, bf16[8,2,64,128]{3,0,1,2:T(8,128)(2,1)}, u32[]{:S(2)}) copy-start(bf16[8,2,64,128]{3,0,1,2:T(8,128)(2,1)} %get-tuple-element.190) | copy-start | bytes 786436
  88.5 13.8 %copy-start.7 = (bf16[8,2,64,128]{3,0,1,2:T(8,128)(2,1)S(1)}, bf16[8,2,64,128]{3,0,1,2:T(8,128)(2,1)}, u32[]{:S(2)}) copy-start(bf16[8,2,64,128]{3,0,1,2:T(8,128)(2,1)} %get-tuple-element.191) | copy-start | bytes 786436
  88.6 51.5 %reduce-scatter.3.cloned.1.call-start = ((), (), s32[]{:S(2)}) async-start(), calls=%async_computation.2 | async-start | bytes 786432 | tf_op jit(solution)/shard_map/reduce_scatter | solution.py:115
  102.7 10.8 %copy-start.3 = (f32[2,8,128,128]{3,2,1,0:T(8,128)S(1)}, f32[2,8,128,128]{3,2,1,0:T(8,128)}, u32[]{:S(2)}) copy-start(f32[2,8,128,128]{3,2,1,0:T(8,128)} %get-tuple-element.126) | copy-start | bytes 3145732
  102.7 10.8 %copy-start.4 = (bf16[8,2,64,128]{3,0,1,2:T(8,128)(2,1)S(1)}, bf16[8,2,64,128]{3,0,1,2:T(8,128)(2,1)}, u32[]{:S(2)}) copy-start(bf16[8,2,64,128]{3,0,1,2:T(8,128)(2,1)} %get-tuple-element.192) | copy-start | bytes 786436
  113.6 1.6 %copy-start.12 = (f32[1024]{0:T(1024)S(1)}, f32[1024]{0:T(1024)}, u32[]{:S(2)}) copy-start(f32[1024]{0:T(1024)} %param.28) | copy-start | bytes 12292
Sparse Core Ops, SparseCore 0:
  15.4 38.6 all-gather.3
  88.7 35.2 reduce-scatter.4
  126.8 13.2 reduce-scatter.2

commit v3 on v2

--- a/solution.py
+++ b/solution.py
@@ -16,31 +16,21 @@
 PRECISION = lax.Precision.DEFAULT
 
 
-def carried_in(array, axis, combine, identity):
+DECAY_ROWS = 16
+
+
+def carried_in(decay, state, axis):
     count, index = (lax.axis_size(axis), lax.axis_index(axis))
-    everything = jax.tree.map(
-        lambda part, kind: lax.all_gather(part.astype(kind), axis),
-        array,
-        (jnp.bfloat16, jnp.bfloat16),
-    )
-    start = jax.tree.map(
-        lambda part, zero: jnp.broadcast_to(jnp.asarray(zero, part.dtype), part.shape),
-        array,
-        identity,
-    )
-
-    def turn(k, before):
-        reached = k < index
-        new = combine(
-            before, jax.tree.map(lambda part, own: part[k].astype(own.dtype), everything, array)
-        )
-        return jax.tree.map(lambda a, b: jnp.where(reached, a, b), new, before)
-
-    return lax.fori_loop(0, count, turn, start)
-
-
-def chain_states(earlier, later):
-    return (earlier[0] * later[0], later[0][..., None] * earlier[1] + later[1])
+    depth = state.shape[1]
+    rows = jnp.broadcast_to(decay[:, None, :], (decay.shape[0], DECAY_ROWS, decay.shape[1]))
+    sent = jnp.concatenate([state, rows], axis=1).astype(jnp.bfloat16)
+    everything = lax.all_gather(sent, axis)
+    before = jnp.zeros_like(state)
+    for k in range(count - 1):
+        part = everything[k].astype(jnp.float32)
+        new = part[:, depth : depth + 1] * before + part[:, :depth]
+        before = jnp.where(k < index, new, before)
+    return before
 
 
 def mixer_half(
@@ -84,7 +74,7 @@
     scores = jnp.where(causal, scores, 0.0)
     within = jnp.einsum("hncs,hnse->hnce", scores, value_heads, precision=PRECISION)
     updates = jnp.einsum(
-        "hncd,hnce->nhde",
+        "hncd,hnce->nhed",
         key_heads * jnp.exp(block_end - cum_decay),
         value_heads,
         precision=PRECISION,
@@ -92,19 +82,18 @@
     block_log = block_end[:, :, 0, :]
     block_decay = jnp.exp(block_log).transpose(1, 0, 2)
 
-    def advance(carry_state, inputs):
-        factor, update = inputs
-        return (factor[..., None] * carry_state + update, carry_state)
-
-    initial = jnp.zeros((head_tensor, HEAD_CHANNELS, HEAD_CHANNELS), jnp.float32)
-    local_final, local_starts = lax.scan(advance, initial, (block_decay, updates))
+    state = jnp.zeros_like(updates[0])
+    starts_list = []
+    for block in range(blocks):
+        starts_list.append(state)
+        state = block_decay[block][:, None, :] * state + updates[block]
+    local_final, local_starts = state, jnp.stack(starts_list)
     device_decay = jnp.exp(jnp.sum(block_log, axis=1))
-    identity = (jnp.ones_like(device_decay), jnp.zeros_like(local_final))
-    _, incoming = carried_in((device_decay, local_final), "ep", chain_states, identity)
+    incoming = carried_in(device_decay, local_final, "ep")
     before = jnp.exp(jnp.cumsum(block_log, axis=1) - block_log).transpose(1, 0, 2)
-    starts = local_starts + before[..., None] * incoming[None]
+    starts = local_starts + before[:, :, None, :] * incoming[None]
     carried = jnp.einsum(
-        "hncd,nhde->hnce", query_heads * jnp.exp(cum_decay), starts, precision=PRECISION
+        "hncd,nhed->hnce", query_heads * jnp.exp(cum_decay), starts, precision=PRECISION
     )
     outputs = (within + carried).transpose(1, 2, 0, 3).reshape(length, head_tensor, HEAD_CHANNELS)
     factor = lax.rsqrt(jnp.mean(outputs * outputs, axis=2, keepdims=True) + EPSILON)
@@ -112,14 +101,16 @@
         None, :
     ]
     gated_rows = (normed * jax.nn.silu(output_gate_input.astype(jnp.float32))).astype(jnp.bfloat16)
-    return lax.psum_scatter(
-        jnp.dot(gated_rows, recurrence_out_weight, preferred_element_type=jnp.float32).astype(
-            jnp.bfloat16
-        ),
-        "tp",
-        scatter_dimension=0,
-        tiled=True,
-    )
+    partial = jnp.dot(
+        gated_rows, recurrence_out_weight, preferred_element_type=jnp.float32
+    ).astype(jnp.bfloat16)
+    if lax.axis_size("tp") != 2:
+        return lax.psum_scatter(partial, "tp", scatter_dimension=0, tiled=True)
+    which, kept_rows = lax.axis_index("tp"), length // 2
+    kept = lax.dynamic_slice_in_dim(partial, which * kept_rows, kept_rows)
+    sent = lax.dynamic_slice_in_dim(partial, (1 - which) * kept_rows, kept_rows)
+    received = lax.ppermute(sent, "tp", [(0, 1), (1, 0)])
+    return (kept.astype(jnp.float32) + received.astype(jnp.float32)).astype(jnp.bfloat16)
 
 
 def expert_half(

time: 147 us -> 136 us (0.925)
  blocking collectives: 12.8 us -> 0 us
  other arithmetic: 19.3 us -> 11 us
  waiting for transfers between devices: 19.2 us -> 24 us
  Pallas kernels: 72.1 us -> 75.2 us
  starting transfers between devices: 0.12 us -> 2.41 us
  local copies, waits for them, and re-layouts: 2.83 us -> 4.37 us
    reduce_scatter x1, waiting for transfers between devices: 4.72 us -> 23.9 us  [dense_expert_half(): total = lax.psum_scatter(routed, 'ep', scatter_dimension=0, tiled=True)]
    reduce_scatter x1 -> x0, waiting for transfers between devices: 14.4 us -> none  [mixer_half(): lax.psum_scatter(jnp.dot(gated_rows, recurrence_out_weight, preferred_ele...]
    all_gather x1 -> x0, blocking collectives: 12.8 us -> none  [carried_in(): lax.all_gather(part.astype(kind), axis)]
    select_n x8 -> x1, other arithmetic: 10.5 us -> 0.42 us  [carried_in(): before = jnp.where(k < index, new, before)]
    pallas_call x1, Pallas kernels: 72.1 us -> 75.2 us  [dense_expert_half(): pl.pallas_call(functools.partial(expert_kernel, count), out_shape=(jax.Sh...]
    ppermute x0 -> x1, starting transfers between devices: none -> 2.33 us  [mixer_half(): received = lax.ppermute(sent, 'tp', [(0, 1), (1, 0)])]
    convert_element_type x10 -> x2, other arithmetic: 0.83 us -> 2.61 us  [the longest x1 1.84 us: carried_in(): part = everything[k].astype(jnp.float32)]
    dynamic_update_slice x2 -> x0, other arithmetic: 1.69 us -> none  [mixer_half(): lax.scan(advance, initial, (block_decay, updates))]
  transfers between devices with their start and end apart: 3 -> 3, of which waited for: 2 -> 1; matrix products, arithmetic and copies ran while one was open for 14% -> 9% of each run, Pallas kernels for 49% -> 55%
where the time goes in v3:
time: 136 us
  Pallas kernels  75.2 us (55%)
  waiting for transfers between devices  24 us (18%)
  between operations  14.5 us (11%)
  other arithmetic  11 us (8%)
  matrix products  4.39 us (3%)
  local copies, waits for them, and re-layouts  4.37 us (3%)
  starting transfers between devices  2.41 us (2%)
    pallas_call x1, Pallas kernels, dense_expert_half(): pl.pallas_call(functools.partial(expert_kernel, count), out_shape=(jax.Sh...  75.2 us
    reduce_scatter x1, waiting for transfers between devices, dense_expert_half(): total = lax.psum_scatter(routed, 'ep', scatter_dimension=0, tiled=True)  23.9 us
    dot_general x1, matrix products, mixer_half(): jnp.dot(gated_rows, recurrence_out_weight, preferred_element_type=jnp.flo...  3.08 us
  transfers between devices with their start and end apart: 3, of which 1 were waited for; matrix products, arithmetic and copies ran while one was open for 9% of the time, Pallas kernels for 55%

profile of v3, /device:TPU:0, one launch (start us, length us, event | category | flops | bytes accessed | tf_op | source)
XLA Modules:
  0.0 135.9 jit_solution(18066084793452295340)
XLA Ops:
  7.2 0.8 copy.72
  8.0 0.2 broadcast_in_dim.23
  8.2 1.3 fusion.51
  9.5 0.1 copy.91
  9.6 0.2 fusion.26
  9.9 0.1 fusion.11
  10.0 0.1 copy.89
  10.2 0.4 copy-done.8
  10.7 1.1 bitcast_multiply_fusion.1
  11.8 0.4 convolution_bitcast_fusion
  12.2 0.9 fusion.25
  13.1 0.7 pad_maximum_fusion
  14.1 0.2 fusion.4
  14.3 0.1 copy.86
  14.4 0.2 fusion.6
  14.6 0.6 subtract_convert_fusion
  15.2 0.9 concatenate.15.x_ref
  16.2 75.2 %expert_kernel.1 = (bf16[1024,1024]{1,0:T(8,128)(2,1)}, f32[128,1024]{1,0:T(8,128)S(1)}) custom-call(bf16[128,2176]{1,0:T(8,128)(2,1)S(1)} %concatenate.15.x_ref, bf16[1,2048,512]{2,1,0:T(8,128)(2,1)S(1)} %copy-done, bf16[1,2048,512]{2,1,0:T(8,128)(2,1)} %up_hbm.1, bf16[1,1024,1024]{2,1,0:T(8,128)(2,1)} %down_hbm.1, bf16[2048,512]{1,0:T(8,128)(2,1)} %shared_gate_hbm.1, ...), custom_call_target="tpu_custom_call" | custom-call | flops 44999999488 | bytes 16000000 | tf_op jit(solution)/shard_map/expert_kernel/pallas_call | solution.py:434
  91.5 0.8 fusion.3
  92.4 0.1 copy-done.7
  92.5 0.4 fusion.1
  92.9 1.8 %fusion.36 = (f32[8,144,128]{2,1,0:T(8,128)S(1)}, f32[8,144,128]{2,1,0:T(8,128)S(1)}, f32[8,144,128]{2,1,0:T(8,128)S(1)}, f32[8,144,128]{2,1,0:T(8,128)S(1)}, f3...) fusion(bf16[8,8,144,128]{3,2,1,0:T(8,128)(2,1)} %all-gather.2.cloned.1.call-done), kind=kLoop, calls=%fused_computation.66 | loop fusion | flops 1032192 | bytes 6193152 | tf_op jit(solution)/shard_map/convert_element_type | solution.py:30
  94.9 0.4 fusion.18
  95.3 0.6 copy-done.3
  96.0 0.6 multiply_reduce_fusion
  96.7 0.3 copy.82
  97.0 0.2 mul.230
  97.2 3.1 %convolution_convert_fusion = bf16[128,2048]{1,0:T(8,128)(2,1)S(1)} fusion(bf16[1024,2048]{1,0:T(8,128)(2,1)} %param.25, bf16[128,1024]{1,0:T(8,128)(2,1)S(1)} %copy-done.12, f32[16,8,8,128]{3,2,1,0:T(8,128)S(1)} %bitcast.136, f32[16,8,8,128]{3,2,1,0:T(8,128)S(1)} %bitcast.137, f32[1024]{0:T(1024)S(1)} %copy-done.13), kind=kOutput, calls=%fused_computation | convolution fusion | flops 538312704 | bytes 6033408 | tf_op jit(solution)/shard_map/dot_general | solution.py:104
  100.3 2.3 %collective-permute-start = (bf16[64,2048]{1,0:T(8,128)(2,1)S(1)}, bf16[64,2048]{1,0:T(8,128)(2,1)S(1)}, u32[]{:S(2)}, u32[]{:S(2)}) collective-permute-start(bf16[64,2048]{1,0:T(8,128)(2,1)S(1)} %constant_dynamic-slice_fusion), channel_id=1, source_target_pairs={{0,1},{1,0},{2,3},{3,2},{4,5},{5,4},{6,7},{7,6},{8,9},{9,8},{10,11... | collective-permute-start | bytes 786440 | tf_op jit(solution)/shard_map/ppermute | solution.py:112
  102.6 23.9 %reduce-scatter.2.cloned.1.call-done = bf16[128,1024]{1,0:T(8,128)(2,1)} async-done(((bf16[1024,1024]{1,0:T(8,128)(2,1)}), bf16[128,1024]{1,0:T(8,128)(2,1)}) %reduce-scatter.2.cloned.1.call-update) | async-done | bytes 262160 | tf_op jit(solution)/shard_map/reduce_scatter | solution.py:476
  126.6 1.7 %add_convert_fusion = bf16[128,1024]{1,0:T(8,128)(2,1)} fusion(f32[128,1024]{1,0:T(8,128)S(1)} %get-tuple-element.4, bf16[128,1024]{1,0:T(8,128)(2,1)} %reduce-scatter.2.cloned.1.call-done), kind=kLoop, calls=%fused_computation.60 | loop fusion | flops 393216 | bytes 1048576 | tf_op jit(solution)/shard_map/convert_element_type | solution.py:477
  128.3 0.8 add_convert_fusion.1
  (56 shorter events, 0.8 us)
Async XLA Ops:
  7.2 85.7 %all-gather.2.cloned.1.call-start = ((), (), s32[]{:S(2)}) async-start(), calls=%async_computation.1 | async-start | bytes 2654208 | tf_op jit(solution)/shard_map/all_gather | solution.py:27
  8.2 1.7 %copy-start.5 = (bf16[128,1024]{1,0:T(8,128)(2,1)S(1)}, bf16[128,1024]{1,0:T(8,128)(2,1)}, u32[]{:S(2)}) copy-start(bf16[128,1024]{1,0:T(8,128)(2,1)} %param.18) | copy-start | bytes 786436
  9.6 1.0 copy-start.8
  9.8 2.0 %copy-start.1 = (f32[8,2,64,128]{3,0,1,2:T(8,128)}, f32[8,2,64,128]{3,0,1,2:T(8,128)S(1)}, u32[]{:S(2)}) copy-start(f32[8,2,64,128]{3,0,1,2:T(8,128)S(1)} %fusion.26) | copy-start | bytes 1572868
  11.8 2.1 %copy-start.10 = (f32[128,4]{0,1:T(4,128)S(1)}, f32[128,4]{0,1:T(4,128)}, u32[]{:S(2)}) copy-start(f32[128,4]{0,1:T(4,128)} %param.28) | copy-start | bytes 6148
  11.8 2.1 %copy-start.11 = (s32[128,4]{0,1:T(4,128)S(1)}, s32[128,4]{0,1:T(4,128)}, u32[]{:S(2)}) copy-start(s32[128,4]{0,1:T(4,128)} %param.27) | copy-start | bytes 6148
  11.8 2.3 %copy-start.2 = (bf16[128,2048]{1,0:T(8,128)(2,1)S(1)}, bf16[128,2048]{1,0:T(8,128)(2,1)}, u32[]{:S(2)}) copy-start(bf16[128,2048]{1,0:T(8,128)(2,1)} %param.26) | copy-start | bytes 1572868
  12.1 2.2 %copy-start.9 = (f32[2048]{0:T(1024)S(1)}, f32[2048]{0:T(1024)}, u32[]{:S(2)}) copy-start(f32[2048]{0:T(1024)} %param.29) | copy-start | bytes 24580
  13.1 3.1 %copy-start = (bf16[1,2048,512]{2,1,0:T(8,128)(2,1)S(1)}, bf16[1,2048,512]{2,1,0:T(8,128)(2,1)}, u32[]{:S(2)}) copy-start(bf16[1,2048,512]{2,1,0:T(8,128)(2,1)} %gate_hbm.1) | copy-start | bytes 6291460
  13.8 112.8 %reduce-scatter.2.cloned.1.call-start = ((), (), s32[]{:S(2)}) async-start(), calls=%async_computation.2 | async-start | bytes 2359296 | tf_op jit(solution)/shard_map/reduce_scatter | solution.py:476
  91.4 1.0 copy-start.6
  91.4 1.1 copy-start.7
  94.8 1.0 copy-start.3
  94.9 1.1 copy-start.4
  95.3 1.9 %copy-start.12 = (bf16[128,1024]{1,0:T(8,128)(2,1)S(1)}, bf16[128,1024]{1,0:T(8,128)(2,1)}, u32[]{:S(2)}) copy-start(bf16[128,1024]{1,0:T(8,128)(2,1)} %param.21) | copy-start | bytes 786436
  95.3 1.9 %copy-start.13 = (f32[1024]{0:T(1024)S(1)}, f32[1024]{0:T(1024)}, u32[]{:S(2)}) copy-start(f32[1024]{0:T(1024)} %param.24) | copy-start | bytes 12292
  100.3 28.0 %collective-permute-start = (bf16[64,2048]{1,0:T(8,128)(2,1)S(1)}, bf16[64,2048]{1,0:T(8,128)(2,1)S(1)}, u32[]{:S(2)}, u32[]{:S(2)}) collective-permute-start(bf16[64,2048]{1,0:T(8,128)(2,1)S(1)} %constant_dynamic-slice_fusion), channel_id=1, source_target_pairs={{0,1},{1,0},{2,3},{3,2},{4,5},{5,4},{6,7},{7,6},{8,9},{9,8},{10,11... | collective-permute-start | bytes 786440 | tf_op jit(solution)/shard_map/ppermute | solution.py:112
Sparse Core Ops, SparseCore 0:
  13.9 42.2 all-gather.1
  91.6 34.9 reduce-scatter.1
